TPU v7x, 32 devices: a whole 2x2x4 slice. The times are simulated.
32 devices in a mesh: ep: 8 (over z, x), tp: 4 (over y, core).
Axes of the slice: x: 2, y: 2, z: 4, core: 2. Of those that a mesh axis runs over, the one named last changes fastest.
Arguments:
- queries: bfloat16 [4096, 2048], P('ep', 'tp'), may hold values from -6 to 6
- keys: bfloat16 [4096, 2048], P('ep', 'tp'), may hold values from -12 to 12
- values: bfloat16 [4096, 2048], P('ep', 'tp'), may hold values from -8 to 8
- key_bias: bfloat16 [4096, 16], P('ep', 'tp'), may hold values from -16 to 0
- out_weight: bfloat16 [2048, 2048], P('tp'), may hold values from -0.1875 to 0.1875
- moe_input: bfloat16 [1024, 2048], P('ep'), may hold values from -6 to 6
- moe_gain: float32 [2048], replicated, may hold values from 0.1 to 1.9
- route_ids: int32 [1024, 2], P('ep'), may hold values from 0 to 7, all different within a row; in each aligned block of 128 rows (0 to 127, 128 to 255, ...) at most 48 rows name the same one
- route_scores: float32 [1024, 2], P('ep'), may hold values from 0.05 to 1
- shared_gate: bfloat16 [2048, 2048], P(None, 'tp'), may hold values from -0.125 to 0.125
- shared_up: bfloat16 [2048, 2048], P(None, 'tp'), may hold values from -0.125 to 0.125
- shared_down: bfloat16 [2048, 2048], P('tp'), may hold values from -0.1875 to 0.1875
- expert_gate: bfloat16 [8, 2048, 2048], P('ep', None, 'tp'), may hold values from -0.125 to 0.125
- expert_up: bfloat16 [8, 2048, 2048], P('ep', None, 'tp'), may hold values from -0.125 to 0.125
- expert_down: bfloat16 [8, 2048, 2048], P('ep', 'tp'), may hold values from -0.1875 to 0.1875
Outputs:
- mixed_tokens: bfloat16 [4096, 2048], P('ep', 'tp')
- expert_mix: bfloat16 [1024, 2048], P('ep', 'tp')
Inputs may be any that keep to these rules, and one draw needn't show every extreme that they name: `route_ids`: each row names 2 different experts. Among the 128 rows of one index of ep no expert is named by more than 48 rows, and in some such block one expert is named by exactly 48 rows.
All inputs are finite; a program needn't handle non-finite values.
Results may differ from a plain program's by a relative error of at most 0.019.
Values may be sent and summed in bfloat16 or wider, within the bound.
A program may use at most 128 MiB of HBM per device.

v0:
```python
import jax
import jax.numpy as jnp
from jax import lax
from jax.sharding import PartitionSpec as P

SEQUENCE_COUNT = 1


EPS_NORM = 1e-06
ROUTED_SCALE = 2.5


def partner_2(array, axis, apart):
    return lax.ppermute(array, axis, [(i, i ^ 1 << apart) for i in range(lax.axis_size(axis))])


def absorb(state, query_heads, piece, visible):
    total, carried = state
    key_piece, value_piece, bias_piece = piece
    span = key_piece.shape[0]
    heads = query_heads.shape[1]
    key_heads = key_piece.reshape(span, heads, -1)
    value_heads = value_piece.reshape(span, heads, -1)
    scale = query_heads.shape[2] ** (-0.5)
    logit = (
        jnp.einsum("qhd,khd->hqk", query_heads, key_heads, preferred_element_type=jnp.float32)
        * scale
    )
    logit = logit + bias_piece.astype(jnp.float32).T[:, None, :]
    keep = jnp.where(visible[None], jax.nn.log_sigmoid(-logit), 0.0)
    stay = lax.cumsum(keep, axis=2, reverse=True) - keep + carried[:, :, None]
    weight = jnp.where(visible[None], jnp.exp(jax.nn.log_sigmoid(logit) + stay), 0.0).astype(
        jnp.bfloat16
    )
    total = total + jnp.einsum(
        "hqk,khd->qhd", weight, value_heads, preferred_element_type=jnp.float32
    )
    return (total, carried + jnp.sum(keep, axis=2))


def fresh_state(query_heads):
    return (
        jnp.zeros(query_heads.shape, jnp.float32),
        jnp.zeros((query_heads.shape[1], query_heads.shape[0]), jnp.float32),
    )


def diagonal(query_heads, piece, offset):
    count = query_heads.shape[0]
    span = piece[0].shape[0]
    key_pos = jnp.arange(span, dtype=jnp.int32)
    query_pos = offset + jnp.arange(count, dtype=jnp.int32)
    visible = key_pos[None, :] < query_pos[:, None]
    return absorb(fresh_state(query_heads), query_heads, piece, visible)


def body(
    queries,
    keys,
    values,
    key_bias,
    out_weight,
    moe_input,
    moe_gain,
    route_ids,
    route_scores,
    shared_gate,
    shared_up,
    shared_down,
    expert_gate,
    expert_up,
    expert_down,
):
    span = queries.shape[0]
    heads = key_bias.shape[1]
    query_heads = queries.reshape(span, heads, -1)
    ep_count = lax.axis_size("ep")
    seq_devices = ep_count // SEQUENCE_COUNT
    own_index = lax.axis_index("ep")
    place = own_index % seq_devices
    own_piece = (keys, values, key_bias)
    half = span // 2
    group_bits = seq_devices.bit_length() - 1

    def mirror(rows):
        for bit in range(group_bits):
            rows = partner_2(rows, "ep", bit)
        return rows

    whole = (
        lax.all_gather(own_piece[0], "ep", axis=0, tiled=True),
        lax.all_gather(own_piece[1], "ep", axis=0, tiled=True),
        lax.all_gather(own_piece[2], "ep", axis=0, tiled=True),
    )
    mirror_place = seq_devices - 1 - place
    mirror_index = own_index - place + mirror_place
    early_rows = query_heads[:half]
    late_rows = mirror(queries[half:]).reshape(half, heads, -1)
    partner = tuple(
        (lax.dynamic_slice_in_dim(member, mirror_index * span, span, 0) for member in whole)
    )
    half_visible = jnp.ones((half, span), jnp.bool_)

    def unchanged(inner):
        return inner

    def visit_both(turn, carry):
        early, late = carry
        early_source = jnp.maximum(own_index - turn, 0)
        late_source = jnp.maximum(mirror_index - turn, 0)
        early_piece = tuple(
            (lax.dynamic_slice_in_dim(member, early_source * span, span, 0) for member in whole)
        )
        late_piece = tuple(
            (lax.dynamic_slice_in_dim(member, late_source * span, span, 0) for member in whole)
        )

        def early_taken(inner):
            return absorb(inner, early_rows, early_piece, half_visible)

        def late_taken(inner):
            return absorb(inner, late_rows, late_piece, half_visible)

        early = lax.cond(place >= turn, early_taken, unchanged, early)
        late = lax.cond(mirror_place >= turn, late_taken, unchanged, late)
        return (early, late)

    early_state, late_state = lax.fori_loop(
        1,
        seq_devices,
        visit_both,
        (diagonal(early_rows, own_piece, 0), diagonal(late_rows, partner, half)),
    )
    early_out = early_state[0].astype(jnp.bfloat16).reshape(half, -1)
    late_out = mirror(late_state[0].astype(jnp.bfloat16).reshape(half, -1))
    heads_out = jnp.concatenate([early_out, late_out], axis=0)
    col_count = out_weight.shape[1] // lax.axis_size("tp")
    token_count = moe_input.shape[0]
    inputs = moe_input.astype(jnp.float32)
    normed = (
        inputs * lax.rsqrt(jnp.mean(inputs * inputs, axis=-1, keepdims=True) + EPS_NORM) * moe_gain
    ).astype(jnp.bfloat16)
    own_cols = lax.dynamic_slice_in_dim(normed, lax.axis_index("tp") * col_count, col_count, 1)
    shared_hidden = (
        jax.nn.silu(jnp.dot(normed, shared_gate, preferred_element_type=jnp.float32))
        * jnp.dot(normed, shared_up, preferred_element_type=jnp.float32)
    ).astype(jnp.bfloat16)
    local_experts = expert_gate.shape[0]
    expert_count = local_experts * ep_count
    topk = route_ids.shape[1]
    capacity = 3 * token_count * topk // (2 * expert_count)
    chosen = route_ids.reshape(-1)
    onehot = (chosen[:, None] == jnp.arange(expert_count, dtype=jnp.int32)[None, :]).astype(
        jnp.int32
    )
    place_in = jnp.sum((jnp.cumsum(onehot, axis=0) - onehot) * onehot, axis=1)
    slot_ids = chosen * capacity + place_in
    send_slots = expert_count * capacity
    matches = (
        slot_ids.reshape(token_count, topk)[None]
        == jnp.arange(send_slots, dtype=jnp.int32)[:, None, None]
    )
    dispatch = jnp.sum(matches.astype(jnp.bfloat16), axis=2)
    outgoing = jnp.dot(dispatch, own_cols, preferred_element_type=jnp.float32).astype(jnp.bfloat16)
    arrived = lax.all_to_all(outgoing, "ep", split_axis=0, concat_axis=0, tiled=True)
    piece = lax.all_gather(arrived, "tp", axis=1, tiled=True)
    width = piece.shape[1]
    grid = piece.reshape(ep_count, local_experts, capacity, width)
    gate_sum = jnp.einsum("secd,edf->secf", grid, expert_gate, preferred_element_type=jnp.float32)
    up_sum = jnp.einsum("secd,edf->secf", grid, expert_up, preferred_element_type=jnp.float32)
    expert_hidden = (jax.nn.silu(gate_sum) * up_sum).astype(jnp.bfloat16)
    routed = jnp.einsum(
        "secf,efd->dsec", expert_hidden, expert_down, preferred_element_type=jnp.float32
    ).reshape(lax.axis_size("tp") * col_count, -1)
    common = jnp.einsum("tf,fd->dt", shared_hidden, shared_down, preferred_element_type=jnp.float32)
    summed = lax.psum_scatter(
        jnp.concatenate(
            [
                jnp.einsum("rh,hd->dr", heads_out, out_weight, preferred_element_type=jnp.float32),
                jnp.concatenate([routed, common], axis=1),
            ],
            axis=1,
        ).astype(jnp.bfloat16),
        "tp",
        scatter_dimension=0,
        tiled=True,
    ).astype(jnp.float32)
    mixer_sum = summed[:, :span]
    expert_sum = summed[:, span:]
    mixed_tokens = mixer_sum.T.astype(jnp.bfloat16)
    routed_sum = expert_sum[:, :send_slots].astype(jnp.bfloat16)
    common_sum = expert_sum[:, send_slots:]
    returned = lax.all_to_all(routed_sum, "ep", split_axis=1, concat_axis=1, tiled=True)
    picked = (
        jnp.take(returned, slot_ids, axis=1)
        .astype(jnp.float32)
        .reshape(col_count, token_count, topk)
    )
    gates = route_scores / jnp.sum(route_scores, axis=-1, keepdims=True) * ROUTED_SCALE
    expert_mix = (common_sum + jnp.sum(picked * gates[None], axis=2)).T.astype(jnp.bfloat16)
    return (mixed_tokens, expert_mix)


def solution(mesh):
    return jax.shard_map(
        body,
        mesh=mesh,
        in_specs=(
            P("ep", "tp"),
            P("ep", "tp"),
            P("ep", "tp"),
            P("ep", "tp"),
            P("tp", None),
            P("ep", None),
            P(),
            P("ep", None),
            P("ep", None),
            P(None, "tp"),
            P(None, "tp"),
            P("tp", None),
            P("ep", None, "tp"),
            P("ep", None, "tp"),
            P("ep", "tp", None),
        ),
        out_specs=(P("ep", "tp"), P("ep", "tp")),
        check_vma=False,
    )
```

profile of v0, /device:TPU:0, one launch (start us, length us, event | category | flops | bytes accessed | tf_op | source)
XLA Modules:
  0.0 466.2 jit_solution(12606968122326971985)
XLA Ops:
  7.2 2.2 copy.119
  13.5 3.0 collective-permute-start
  20.2 4.9 %all-to-all-start = ((bf16[8,48,512]{2,1,0:T(8,128)(2,1)}), bf16[8,48,512]{2,1,0:T(8,128)(2,1)S(1)}, u32[]{:S(2)}, u32[]{:S(2)}) async-start(bf16[8,48,512]{2,1,0:T(8,128)(2,1)} %bitcast.32), calls=%async_computation | async-start | bytes 786432 | tf_op jit(solution)/shard_map/all_to_all | solution.py:165
  27.0 2.9 fusion.99
  29.9 3.2 reshape.261
  33.1 4.1 copy.115
  37.2 10.2 %fusion.104 = f32[4,256,4,128]{1,2,3,0:T(4,128)S(1)} fusion(f32[4,256,4,128]{1,2,3,0:T(4,128)} %copy.115), kind=kOutput, calls=%fused_computation.169 | output fusion | flops 66584576 | bytes 4194304 | tf_op jit(solution)/shard_map/reduce-window.4
  51.4 3.3 broadcast_add_fusion.3
  54.7 4.2 copy.116
  58.9 3.6 reduce_window_sum.66
  62.5 6.4 %convolution_bitcast_fusion.3 = f32[256,4,128]{2,0,1:T(8,128)} fusion(f32[4,256,512]{2,1,0:T(8,128)} %reduce_window_sum.66, f32[4,256,512]{2,1,0:T(8,128)} %copy-done.10, pred[256,512]{1,0:T(8,128)(4,1)S(1)} %iota_compare_fusion.1, u8[256,512]{1,0:T(8,128)(4,1)S(1)} %get-tuple-element.558, bf16[512,512]{1,0:T(8,128)(2,1)} %param.23), kind=kOutput, calls=%fused_computation.104 | convolution fusion | flops 146276352 | bytes 5505024 | tf_op jit(solution)/shard_map/hqk,khd->qhd/dot_general | solution.py:35
  69.4 31.9 %all_gather.14 = bf16[4096,4]{0,1:T(4,128)(2,1)S(1)} all-gather(bf16[512,4]{0,1:T(4,128)(2,1)S(1)} %copy-done.20), channel_id=1, replica_groups=mesh['ep'=8,'tp'=4] {'ep'}, dimensions={0}, use_global_device_ids=true | all-gather | bytes 36864 | tf_op jit(solution)/shard_map/all_gather | solution.py:93
  102.5 4.2 fusion.30
  106.6 10.7 %collective-permute-done.1 = bf16[256,512]{0,1:T(8,128)(2,1)} collective-permute-done((bf16[256,512]{0,1:T(8,128)(2,1)}, bf16[256,512]{0,1:T(8,128)(2,1)}, u32[]{:S(2)}, u32[]{:S(2)}) %collective-permute-start.1) | collective-permute-done | bytes 262176 | tf_op jit(solution)/shard_map/ppermute | solution.py:14
  118.5 15.5 %collective-permute-done.2 = bf16[256,512]{0,1:T(8,128)(2,1)S(1)} collective-permute-done((bf16[256,512]{0,1:T(8,128)(2,1)}, bf16[256,512]{0,1:T(8,128)(2,1)S(1)}, u32[]{:S(2)}, u32[]{:S(2)}) %collective-permute-start.2) | collective-permute-done | bytes 262176 | tf_op jit(solution)/shard_map/ppermute | solution.py:14
  135.9 3.6 fusion.100
  139.6 3.1 reshape.267
  142.6 4.2 copy.124
  146.8 10.2 %fusion.105 = f32[4,256,4,128]{1,2,3,0:T(4,128)S(1)} fusion(f32[4,256,4,128]{1,2,3,0:T(4,128)} %copy.124), kind=kOutput, calls=%fused_computation.170 | output fusion | flops 66584576 | bytes 4194304 | tf_op jit(solution)/shard_map/reduce-window.6
  158.4 3.3 broadcast_add_fusion.2
  161.7 4.1 copy.125
  165.8 3.4 reduce_window_sum.68
  169.2 10.9 %all-gather.4.cloned.1.call-done = bf16[4096,512]{0,1:T(8,128)(2,1)} async-done(((bf16[512,512]{0,1:T(8,128)(2,1)}), bf16[4096,512]{0,1:T(8,128)(2,1)}) %all-gather.4.cloned.1.call-update) | async-done | bytes 4194320 | tf_op jit(solution)/shard_map/all_gather | solution.py:92
  181.3 5.4 %convolution_bitcast_fusion.2 = f32[256,4,128]{0,2,1:T(8,128)S(1)} fusion(bf16[512,4,128]{0,2,1:T(8,128)(2,1)S(1)} %bitcast.242, f32[4,256,512]{2,1,0:T(8,128)} %reduce_window_sum.68, f32[4,512,256]{1,2,0:T(8,128)} %get-tuple-element.560, f32[4,512]{1,0:T(4,128)S(1)} %copy-done.24, pred[256,512]{1,0:T(8,128)(4,1)S(1)} %iota_compare_fusion), kind=kOutput, calls=%fused_computation.103 | convolution fusion | flops 145752064 | bytes 5382144 | tf_op jit(solution)/shard_map/hqk,khd->qhd/dot_general | solution.py:35
  186.9 171.1 %while.19 = (s32[]{:T(128)}, f32[256,4,128]{2,0,1:T(8,128)}, f32[4,256]{1,0:T(4,128)S(1)}, f32[256,4,128]{2,0,1:T(8,128)S(1)}, f32[4,256]{1,0:T(4,128)S(1)}, /*i...) while((s32[]{:T(128)}, f32[256,4,128]{2,0,1:T(8,128)}, ...), condition=%wide.region_17.18_spmd, body=%wide.region_6.17_spmd.sunk | while | flops 703893504 | bytes 94184160 | solution.py:128
  189.3 23.3 %conditional.5 = ((f32[256,4,128]{2,0,1:T(8,128)S(1)}, f32[4,256]{1,0:T(4,128)S(1)})) conditional(s32[]{:T(128)} %convert_element_type.140, (f32[256,4,128]{2,0,1:T(8,128)S(1)}, f32[4,256]{1,0:T(4,128)S(1)}) %tuple.82, (s32[]{:T(128)}, s32[]{:T(128)}, bf16[4096,512]{0,1:T(8,128)(2,1)}, bf16[256,4,128]{2,0,1:T(8,128)(2,1)}, ...), branch_computations={%region_12.12_spmd, %region_13.16_spmd} | conditional | flops 351946752 | bytes 45519040 | solution.py:125
  191.3 2.9 fusion.26
  194.2 9.6 %fusion.23 = f32[4,256,4,128]{1,2,3,0:T(4,128)S(1)} fusion(f32[4,256,4,128]{1,3,2,0:T(8,128)S(1)} %bitcast.233), kind=kOutput, calls=%fused_computation.44 | output fusion | flops 66584576 | bytes 4194304 | tf_op jit(solution)/shard_map/reduce-window.20
  208.7 3.2 fusion.17
  212.7 23.3 %conditional.5 = ((f32[256,4,128]{2,0,1:T(8,128)S(1)}, f32[4,256]{1,0:T(4,128)S(1)})) conditional(s32[]{:T(128)} %convert_element_type.140, (f32[256,4,128]{2,0,1:T(8,128)S(1)}, f32[4,256]{1,0:T(4,128)S(1)}) %tuple.82, (s32[]{:T(128)}, s32[]{:T(128)}, bf16[4096,512]{0,1:T(8,128)(2,1)}, bf16[256,4,128]{2,0,1:T(8,128)(2,1)}, ...), branch_computations={%region_12.12_spmd, %region_13.16_spmd} | conditional | flops 351946752 | bytes 45519040 | solution.py:125
  214.7 2.9 fusion.26
  217.6 9.6 %fusion.23 = f32[4,256,4,128]{1,2,3,0:T(4,128)S(1)} fusion(f32[4,256,4,128]{1,3,2,0:T(8,128)S(1)} %bitcast.233), kind=kOutput, calls=%fused_computation.44 | output fusion | flops 66584576 | bytes 4194304 | tf_op jit(solution)/shard_map/reduce-window.20
  232.1 3.2 fusion.17
  236.0 23.3 %conditional.5 = ((f32[256,4,128]{2,0,1:T(8,128)S(1)}, f32[4,256]{1,0:T(4,128)S(1)})) conditional(s32[]{:T(128)} %convert_element_type.140, (f32[256,4,128]{2,0,1:T(8,128)S(1)}, f32[4,256]{1,0:T(4,128)S(1)}) %tuple.82, (s32[]{:T(128)}, s32[]{:T(128)}, bf16[4096,512]{0,1:T(8,128)(2,1)}, bf16[256,4,128]{2,0,1:T(8,128)(2,1)}, ...), branch_computations={%region_12.12_spmd, %region_13.16_spmd} | conditional | flops 351946752 | bytes 45519040 | solution.py:125
  238.1 2.9 fusion.26
  241.0 9.6 %fusion.23 = f32[4,256,4,128]{1,2,3,0:T(4,128)S(1)} fusion(f32[4,256,4,128]{1,3,2,0:T(8,128)S(1)} %bitcast.233), kind=kOutput, calls=%fused_computation.44 | output fusion | flops 66584576 | bytes 4194304 | tf_op jit(solution)/shard_map/reduce-window.20
  255.5 3.2 fusion.17
  259.4 23.3 %conditional.5 = ((f32[256,4,128]{2,0,1:T(8,128)S(1)}, f32[4,256]{1,0:T(4,128)S(1)})) conditional(s32[]{:T(128)} %convert_element_type.140, (f32[256,4,128]{2,0,1:T(8,128)S(1)}, f32[4,256]{1,0:T(4,128)S(1)}) %tuple.82, (s32[]{:T(128)}, s32[]{:T(128)}, bf16[4096,512]{0,1:T(8,128)(2,1)}, bf16[256,4,128]{2,0,1:T(8,128)(2,1)}, ...), branch_computations={%region_12.12_spmd, %region_13.16_spmd} | conditional | flops 351946752 | bytes 45519040 | solution.py:125
  261.5 2.9 fusion.26
  264.4 9.6 %fusion.23 = f32[4,256,4,128]{1,2,3,0:T(4,128)S(1)} fusion(f32[4,256,4,128]{1,3,2,0:T(8,128)S(1)} %bitcast.233), kind=kOutput, calls=%fused_computation.44 | output fusion | flops 66584576 | bytes 4194304 | tf_op jit(solution)/shard_map/reduce-window.20
  278.9 3.2 fusion.17
  282.8 23.3 %conditional.5 = ((f32[256,4,128]{2,0,1:T(8,128)S(1)}, f32[4,256]{1,0:T(4,128)S(1)})) conditional(s32[]{:T(128)} %convert_element_type.140, (f32[256,4,128]{2,0,1:T(8,128)S(1)}, f32[4,256]{1,0:T(4,128)S(1)}) %tuple.82, (s32[]{:T(128)}, s32[]{:T(128)}, bf16[4096,512]{0,1:T(8,128)(2,1)}, bf16[256,4,128]{2,0,1:T(8,128)(2,1)}, ...), branch_computations={%region_12.12_spmd, %region_13.16_spmd} | conditional | flops 351946752 | bytes 45519040 | solution.py:125
  284.9 2.9 fusion.26
  287.7 9.6 %fusion.23 = f32[4,256,4,128]{1,2,3,0:T(4,128)S(1)} fusion(f32[4,256,4,128]{1,3,2,0:T(8,128)S(1)} %bitcast.233), kind=kOutput, calls=%fused_computation.44 | output fusion | flops 66584576 | bytes 4194304 | tf_op jit(solution)/shard_map/reduce-window.20
  302.3 3.2 fusion.17
  306.2 23.3 %conditional.5 = ((f32[256,4,128]{2,0,1:T(8,128)S(1)}, f32[4,256]{1,0:T(4,128)S(1)})) conditional(s32[]{:T(128)} %convert_element_type.140, (f32[256,4,128]{2,0,1:T(8,128)S(1)}, f32[4,256]{1,0:T(4,128)S(1)}) %tuple.82, (s32[]{:T(128)}, s32[]{:T(128)}, bf16[4096,512]{0,1:T(8,128)(2,1)}, bf16[256,4,128]{2,0,1:T(8,128)(2,1)}, ...), branch_computations={%region_12.12_spmd, %region_13.16_spmd} | conditional | flops 351946752 | bytes 45519040 | solution.py:125
  308.3 2.9 fusion.26
  311.1 9.6 %fusion.23 = f32[4,256,4,128]{1,2,3,0:T(4,128)S(1)} fusion(f32[4,256,4,128]{1,3,2,0:T(8,128)S(1)} %bitcast.233), kind=kOutput, calls=%fused_computation.44 | output fusion | flops 66584576 | bytes 4194304 | tf_op jit(solution)/shard_map/reduce-window.20
  325.7 3.2 fusion.17
  329.6 23.3 %conditional.5 = ((f32[256,4,128]{2,0,1:T(8,128)S(1)}, f32[4,256]{1,0:T(4,128)S(1)})) conditional(s32[]{:T(128)} %convert_element_type.140, (f32[256,4,128]{2,0,1:T(8,128)S(1)}, f32[4,256]{1,0:T(4,128)S(1)}) %tuple.82, (s32[]{:T(128)}, s32[]{:T(128)}, bf16[4096,512]{0,1:T(8,128)(2,1)}, bf16[256,4,128]{2,0,1:T(8,128)(2,1)}, ...), branch_computations={%region_12.12_spmd, %region_13.16_spmd} | conditional | flops 351946752 | bytes 45519040 | solution.py:125
  331.7 2.9 fusion.26
  334.5 9.6 %fusion.23 = f32[4,256,4,128]{1,2,3,0:T(4,128)S(1)} fusion(f32[4,256,4,128]{1,3,2,0:T(8,128)S(1)} %bitcast.233), kind=kOutput, calls=%fused_computation.44 | output fusion | flops 66584576 | bytes 4194304 | tf_op jit(solution)/shard_map/reduce-window.20
  349.1 3.2 fusion.17
  358.1 3.5 collective-permute-start.3
  361.6 3.2 fusion.52
  366.0 2.5 collective-permute-start.4
  369.5 4.8 %collective-permute-done.4 = bf16[256,512]{0,1:T(8,128)(2,1)S(1)} collective-permute-done((bf16[256,512]{0,1:T(8,128)(2,1)S(1)}, bf16[256,512]{0,1:T(8,128)(2,1)S(1)}, u32[]{:S(2)}, u32[]{:S(2)}) %collective-permute-start.4) | collective-permute-done | bytes 262176 | tf_op jit(solution)/shard_map/ppermute | solution.py:14
  374.3 5.8 %collective-permute-start.5 = (bf16[256,512]{0,1:T(8,128)(2,1)S(1)}, bf16[256,512]{0,1:T(8,128)(2,1)S(1)}, u32[]{:S(2)}, u32[]{:S(2)}) collective-permute-start(bf16[256,512]{0,1:T(8,128)(2,1)S(1)} %collective-permute-done.4), channel_id=1, source_target_pairs={{0,16},{4,20},{8,24},{12,28},{16,0},{20,4},{24,8},{28,12},{1,17},{... | collective-permute-start | bytes 786440 | tf_op jit(solution)/shard_map/ppermute | solution.py:14
  380.1 2.1 fusion.29
  382.4 4.9 %collective-permute-done.5 = bf16[256,512]{0,1:T(8,128)(2,1)S(1)} collective-permute-done((bf16[256,512]{0,1:T(8,128)(2,1)S(1)}, bf16[256,512]{0,1:T(8,128)(2,1)S(1)}, u32[]{:S(2)}, u32[]{:S(2)}) %collective-permute-start.5) | collective-permute-done | bytes 262176 | tf_op jit(solution)/shard_map/ppermute | solution.py:14
  388.9 2.2 pad_maximum_fusion
  392.4 44.3 %reduce-scatter.2.cloned.1.call-done = bf16[512,1024]{0,1:T(8,128)(2,1)} async-done(((bf16[2048,1024]{0,1:T(8,128)(2,1)}), bf16[512,1024]{0,1:T(8,128)(2,1)}) %reduce-scatter.2.cloned.1.call-update) | async-done | bytes 1048592 | tf_op jit(solution)/shard_map/reduce_scatter | solution.py:176
  438.6 5.5 %all-to-all-start.1 = ((bf16[512,8,48]{0,2,1:T(8,128)(2,1)}), bf16[512,8,48]{0,2,1:T(8,128)(2,1)S(1)}, u32[]{:S(2)}, u32[]{:S(2)}) async-start(bf16[512,8,48]{0,2,1:T(8,128)(2,1)} %bitcast.52), calls=%async_computation.2 | async-start | bytes 786432 | tf_op jit(solution)/shard_map/all_to_all | solution.py:193
  450.7 4.9 %all-to-all-done.1 = bf16[512,8,48]{0,2,1:T(8,128)(2,1)S(1)} async-done(((bf16[512,8,48]{0,2,1:T(8,128)(2,1)}), bf16[512,8,48]{0,2,1:T(8,128)(2,1)S(1)}, u32[]{:S(2)}, u32[]{:S(2)}) %all-to-all-start.1) | async-done | bytes 393248 | tf_op jit(solution)/shard_map/all_to_all | solution.py:193
  (229 shorter events, 91.5 us)
Async XLA Ops:
  7.2 380.1 %copy-start = (bf16[512,2048]{1,0:T(8,128)(2,1)S(1)}, bf16[512,2048]{1,0:T(8,128)(2,1)}, u32[]{:S(2)}) copy-start(bf16[512,2048]{1,0:T(8,128)(2,1)} %param.25) | copy-start | bytes 6291460
  7.2 127.7 %all-gather.6.cloned.1.call-start = ((), (), s32[]{:S(2)}) async-start(), calls=%async_computation.4 | async-start | bytes 4718592 | tf_op jit(solution)/shard_map/all_gather | solution.py:91
  9.4 7.1 %copy-start.21 = (s32[128,2]{0,1:T(2,128)S(1)}, s32[128,2]{0,1:T(2,128)}, u32[]{:S(2)}) copy-start(s32[128,2]{0,1:T(2,128)} %param.28) | copy-start | bytes 3076
  9.4 9.3 %copy-start.12 = (bf16[128,2048]{1,0:T(8,128)(2,1)S(1)}, bf16[128,2048]{1,0:T(8,128)(2,1)}, u32[]{:S(2)}) copy-start(bf16[128,2048]{1,0:T(8,128)(2,1)} %param.26) | copy-start | bytes 1572868
  9.4 9.5 %copy-start.23 = (f32[2048]{0:T(1024)S(1)}, f32[2048]{0:T(1024)}, u32[]{:S(2)}) copy-start(f32[2048]{0:T(1024)} %param.27) | copy-start | bytes 24580
  9.4 170.7 %all-gather.4.cloned.1.call-start = ((), (), s32[]{:S(2)}) async-start(), calls=%async_computation.3 | async-start | bytes 4718592 | tf_op jit(solution)/shard_map/all_gather | solution.py:92
  13.5 11.7 %copy-start.20 = (bf16[512,4]{0,1:T(4,128)(2,1)S(1)}, bf16[512,4]{0,1:T(4,128)(2,1)}, u32[]{:S(2)}) copy-start(bf16[512,4]{0,1:T(4,128)(2,1)} %param.24) | copy-start | bytes 12292
  13.5 89.0 %collective-permute-start = (bf16[256,512]{0,1:T(8,128)(2,1)}, bf16[256,512]{0,1:T(8,128)(2,1)}, u32[]{:S(2)}, u32[]{:S(2)}) collective-permute-start(bf16[256,512]{0,1:T(8,128)(2,1)} %copy.148), channel_id=1, source_target_pairs={{0,4},{4,0},{8,12},{12,8},{16,20},{20,16},{24,28},{28,24},{1,5},{5... | collective-permute-start | bytes 786440 | tf_op jit(solution)/shard_map/ppermute | solution.py:14
  17.9 9.2 %copy-start.22 = (s32[256]{0:T(256)}, s32[256]{0:T(256)S(1)}, u32[]{:S(2)}) copy-start(s32[256]{0:T(256)S(1)} %fusion.90) | copy-start | bytes 3076
  20.2 97.3 %all-to-all-start = ((bf16[8,48,512]{2,1,0:T(8,128)(2,1)}), bf16[8,48,512]{2,1,0:T(8,128)(2,1)S(1)}, u32[]{:S(2)}, u32[]{:S(2)}) async-start(bf16[8,48,512]{2,1,0:T(8,128)(2,1)} %bitcast.32), calls=%async_computation | async-start | bytes 786432 | tf_op jit(solution)/shard_map/all_to_all | solution.py:165
  25.0 336.6 %all-gather.8.cloned.1.call-start = ((), (), s32[]{:S(2)}) async-start(), calls=%async_computation.5 | async-start | bytes 1966080 | tf_op jit(solution)/shard_map/all_gather | solution.py:166
  27.0 2.9 copy-start.10
  47.4 1.3 copy-start.8
  62.5 6.4 %copy-start.11 = (bf16[2048,512]{1,0:T(8,128)(2,1)S(1)}, bf16[2048,512]{1,0:T(8,128)(2,1)}, u32[]{:S(2)}) copy-start(bf16[2048,512]{1,0:T(8,128)(2,1)} %param.30) | copy-start | bytes 6291460
  101.3 0.6 copy-start.19
  102.5 14.8 %collective-permute-start.1 = (bf16[256,512]{0,1:T(8,128)(2,1)}, bf16[256,512]{0,1:T(8,128)(2,1)}, u32[]{:S(2)}, u32[]{:S(2)}) collective-permute-start(bf16[256,512]{0,1:T(8,128)(2,1)} %collective-permute-done), channel_id=1, source_target_pairs={{0,8},{4,12},{8,0},{12,4},{16,24},{20,28},{24,16},{28,20},{1,9},{5... | collective-permute-start | bytes 786440 | tf_op jit(solution)/shard_map/ppermute | solution.py:14
  106.6 29.3 %copy-start.24 = (f32[4,512]{1,0:T(4,128)S(1)}, f32[4,512]{1,0:T(4,128)}, u32[]{:S(2)}) copy-start(f32[4,512]{1,0:T(4,128)} %convert_bitcast_fusion.2) | copy-start | bytes 24580
  117.3 16.7 %collective-permute-start.2 = (bf16[256,512]{0,1:T(8,128)(2,1)}, bf16[256,512]{0,1:T(8,128)(2,1)S(1)}, u32[]{:S(2)}, u32[]{:S(2)}) collective-permute-start(bf16[256,512]{0,1:T(8,128)(2,1)} %collective-permute-done.1), channel_id=1, source_target_pairs={{0,16},{4,20},{8,24},{12,28},{16,0},{20,4},{24,8},{28,12},{1,17},{... | collective-permute-start | bytes 786440 | tf_op jit(solution)/shard_map/ppermute | solution.py:14
  117.5 0.8 copy-start.15
  118.3 318.4 %reduce-scatter.2.cloned.1.call-start = ((), (), s32[]{:S(2)}) async-start(), calls=%async_computation.6 | async-start | bytes 5242880 | tf_op jit(solution)/shard_map/reduce_scatter | solution.py:176
  157.0 1.3 copy-start.9
  189.3 2.0 copy-start.18
  203.8 1.3 copy-start.1
  207.2 1.6 copy-start.3
  212.7 2.0 copy-start.18
  227.2 1.3 copy-start.1
  230.5 1.6 copy-start.3
  236.1 2.0 copy-start.18
  250.6 1.3 copy-start.1
  253.9 1.6 copy-start.3
  259.5 2.0 copy-start.18
  274.0 1.3 copy-start.1
  277.3 1.6 copy-start.3
  282.9 2.0 copy-start.18
  297.4 1.3 copy-start.1
  300.7 1.6 copy-start.3
  306.2 2.0 copy-start.18
  320.8 1.3 copy-start.1
  324.1 1.6 copy-start.3
  329.6 2.0 copy-start.18
  344.2 1.3 copy-start.1
  347.5 1.6 copy-start.3
  358.1 7.8 %collective-permute-start.3 = (bf16[256,512]{0,1:T(8,128)(2,1)S(1)}, bf16[256,512]{0,1:T(8,128)(2,1)S(1)}, u32[]{:S(2)}, u32[]{:S(2)}) collective-permute-start(bf16[256,512]{0,1:T(8,128)(2,1)S(1)} %bitcast.244), channel_id=1, source_target_pairs={{0,4},{4,0},{8,12},{12,8},{16,20},{20,16},{24,28},{28,24},{1,5},{5... | collective-permute-start | bytes 786440 | tf_op jit(solution)/shard_map/ppermute | solution.py:14
  361.6 6.8 %copy-start.26 = (bf16[1,2048,512]{2,1,0:T(8,128)(2,1)S(1)}, bf16[1,2048,512]{2,1,0:T(8,128)(2,1)}, u32[]{:S(2)}) copy-start(bf16[1,2048,512]{2,1,0:T(8,128)(2,1)} %param.34) | copy-start | bytes 6291460
  361.6 6.8 %copy-start.28 = (bf16[384,2048]{1,0:T(8,128)(2,1)S(1)}, bf16[384,2048]{1,0:T(8,128)(2,1)}, u32[]{:S(2)}) copy-start(bf16[384,2048]{1,0:T(8,128)(2,1)} %all-gather.8.cloned.1.call-done) | copy-start | bytes 4718596
  364.8 15.3 %copy-start.27 = (bf16[1,512,2048]{2,1,0:T(8,128)(2,1)S(1)}, bf16[1,512,2048]{2,1,0:T(8,128)(2,1)}, u32[]{:S(2)}) copy-start(bf16[1,512,2048]{2,1,0:T(8,128)(2,1)} %param.35) | copy-start | bytes 6291460
  366.0 8.4 %collective-permute-start.4 = (bf16[256,512]{0,1:T(8,128)(2,1)S(1)}, bf16[256,512]{0,1:T(8,128)(2,1)S(1)}, u32[]{:S(2)}, u32[]{:S(2)}) collective-permute-start(bf16[256,512]{0,1:T(8,128)(2,1)S(1)} %collective-permute-done.3), channel_id=1, source_target_pairs={{0,8},{4,12},{8,0},{12,4},{16,24},{20,28},{24,16},{28,20},{1,9},{5... | collective-permute-start | bytes 786440 | tf_op jit(solution)/shard_map/ppermute | solution.py:14
  374.3 13.0 %collective-permute-start.5 = (bf16[256,512]{0,1:T(8,128)(2,1)S(1)}, bf16[256,512]{0,1:T(8,128)(2,1)S(1)}, u32[]{:S(2)}, u32[]{:S(2)}) collective-permute-start(bf16[256,512]{0,1:T(8,128)(2,1)S(1)} %collective-permute-done.4), channel_id=1, source_target_pairs={{0,16},{4,20},{8,24},{12,28},{16,0},{20,4},{24,8},{28,12},{1,17},{... | collective-permute-start | bytes 786440 | tf_op jit(solution)/shard_map/ppermute | solution.py:14
  380.1 2.1 copy-start.7
  387.3 1.3 copy-start.13
  387.3 1.6 copy-start.14
  391.1 0.7 copy-start.25
  436.7 13.2 %copy-start.16 = (bf16[512,1024]{0,1:T(8,128)(2,1)S(1)}, bf16[512,1024]{0,1:T(8,128)(2,1)}, u32[]{:S(2)}) copy-start(bf16[512,1024]{0,1:T(8,128)(2,1)} %reduce-scatter.2.cloned.1.call-done) | copy-start | bytes 3145732
  438.6 17.1 %all-to-all-start.1 = ((bf16[512,8,48]{0,2,1:T(8,128)(2,1)}), bf16[512,8,48]{0,2,1:T(8,128)(2,1)S(1)}, u32[]{:S(2)}, u32[]{:S(2)}) async-start(bf16[512,8,48]{0,2,1:T(8,128)(2,1)} %bitcast.52), calls=%async_computation.2 | async-start | bytes 786432 | tf_op jit(solution)/shard_map/all_to_all | solution.py:193
  450.7 6.3 %copy-start.17 = (f32[128,2]{1,0:T(8,128)S(1)}, f32[128,2]{1,0:T(8,128)}, u32[]{:S(2)}) copy-start(f32[128,2]{1,0:T(8,128)} %copy.136) | copy-start | bytes 3076
Sparse Core Ops, SparseCore 0:
  10.0 86.2 all-gather.5
  98.3 81.8 all-gather.3
  181.8 17.8 all-gather.7
  391.2 45.4 reduce-scatter.1
where the time goes:
time: 472 us; the launch traced here: 466 us
  other arithmetic  149 us (32%)
  waiting for transfers between devices  97.3 us (21%)
  local copies, waits for them, and re-layouts  85 us (18%)
  matrix products  54.8 us (12%)
  blocking collectives  31.9 us (7%)
  starting transfers between devices  25.3 us (5%)
  between operations  14.3 us (3%)
  loops' own time  8.35 us (2%)
    another operation x20, other arithmetic  90.1 us
    reduce_scatter x1, waiting for transfers between devices, body(): lax.psum_scatter(jnp.concatenate([jnp.einsum('rh,hd->dr', heads_out, out_...  44.3 us
    ppermute x6, waiting for transfers between devices, partner_2(): lax.ppermute(array, axis, [(i, i ^ 1 << apart) for i in range(lax.axis_si...  37 us
    all_gather x1, blocking collectives, body(): lax.all_gather(own_piece[2], 'ep', axis=0, tiled=True)  31.9 us
    dot_general x9, matrix products, absorb(): jnp.einsum('qhd,khd->hqk', query_heads, key_heads, preferred_element_type...  25.4 us
    convert_element_type x7, other arithmetic, absorb(): jnp.where(visible[None], jnp.exp(jax.nn.log_sigmoid(logit) + stay), 0.0)  22.5 us
    another operation x9, other arithmetic, absorb(): stay = lax.cumsum(keep, axis=2, reverse=True) - keep + carried[:, :, None]  20.3 us
    another operation x11, local copies, waits for them, and re-layouts, absorb(): stay = lax.cumsum(keep, axis=2, reverse=True) - keep + carried[:, :, None]  17.9 us
  transfers between devices with their start and end apart: 12, of which 8 were waited for; matrix products, arithmetic and copies ran while one was open for 55% of the time, Pallas kernels for 0%

commit v1 on v0

v1 whole, which is shorter than its diff:
```python
import functools

import jax
import jax.numpy as jnp
from jax import lax
from jax.experimental import pallas as pl
from jax.experimental.pallas import tpu as pltpu
from jax.sharding import PartitionSpec as P

EPS_NORM = 1e-06
ROUTED_SCALE = 2.5
LOG2E = 1.4426950408889634
BIAS_ROWS = 16


def attention_kernel(share, span, place_ref, data_ref, tri_ref, out_ref):
    block = pl.program_id(0)
    offset = place_ref[0] * share
    width = tri_ref.shape[0]
    size = out_ref.shape[2]
    query = data_ref[block, pl.ds(0, share), :]
    scale = size ** (-0.5) * LOG2E

    def unit(key_block, carry, masked):
        total, passed = carry
        key = data_ref[key_block, pl.ds(share, span), :]
        value = data_ref[key_block, pl.ds(share + span, span), :]
        bias = data_ref[key_block, pl.ds(share + 2 * span, BIAS_ROWS), :].astype(jnp.float32)
        bias = bias * LOG2E
        for start in range(span - width, -1, -width):
            row = jnp.concatenate(
                [
                    bias[i : i + 1, :]
                    for i in range(start // size, (start + width) // size)
                ],
                axis=1,
            )
            logit = (
                lax.dot_general(
                    query,
                    key[start : start + width],
                    (((1,), (1,)), ((), ())),
                    preferred_element_type=jnp.float32,
                )
                * scale
                + row
            )
            drop = jnp.maximum(logit, jnp.log(1.0 + jnp.exp2(jnp.minimum(logit, 126.0))) * LOG2E)
            base = logit - drop
            if masked:
                shape = (share, width)
                visible = start + lax.broadcasted_iota(
                    jnp.int32, shape, 1
                ) < offset + lax.broadcasted_iota(jnp.int32, shape, 0)
                drop = jnp.where(visible, drop, 0.0)
            later = jnp.dot(
                drop.astype(jnp.bfloat16), tri_ref[...], preferred_element_type=jnp.float32
            )
            weight = jnp.exp2(base - later - passed)
            if masked:
                weight = jnp.where(visible, weight, 0.0)
            passed = passed + later[:, 0:1] + drop[:, 0:1]
            total = total + jnp.dot(
                weight.astype(jnp.bfloat16),
                value[start : start + width],
                preferred_element_type=jnp.float32,
            )
        return (total, passed)

    carry = (jnp.zeros((share, size), jnp.float32), jnp.zeros((share, 1), jnp.float32))
    carry = unit(block, carry, True)
    carry = lax.fori_loop(0, block, lambda i, c: unit(block - 1 - i, c, False), carry)
    out_ref[0] = carry[0].astype(out_ref.dtype)


def attention(data, place, share, span):
    blocks, _, size = data.shape
    width = min(256, span)
    index = jnp.arange(width)
    tri = (index[:, None] > index[None, :]).astype(jnp.bfloat16)
    work = blocks * (blocks + 1) // 2 * share * span
    return pl.pallas_call(
        functools.partial(attention_kernel, share, span),
        grid=(blocks,),
        in_specs=[
            pl.BlockSpec(memory_space=pltpu.SMEM),
            pl.BlockSpec(memory_space=pltpu.VMEM),
            pl.BlockSpec(memory_space=pltpu.VMEM),
        ],
        out_specs=pl.BlockSpec((1, share, size), lambda i: (i, 0, 0)),
        out_shape=jax.ShapeDtypeStruct((blocks, share, size), jnp.bfloat16),
        cost_estimate=pl.CostEstimate(
            flops=work * (4 * size + 2 * width),
            bytes_accessed=data.size * 2,
            transcendentals=3 * work,
        ),
        compiler_params=pltpu.CompilerParams(
            dimension_semantics=("arbitrary",), vmem_limit_bytes=40 * 1024 * 1024
        ),
        name="stick",
    )(place, data, tri)


def body(
    queries,
    keys,
    values,
    key_bias,
    out_weight,
    moe_input,
    moe_gain,
    route_ids,
    route_scores,
    shared_gate,
    shared_up,
    shared_down,
    expert_gate,
    expert_up,
    expert_down,
):
    span = queries.shape[0]
    heads = key_bias.shape[1]
    size = queries.shape[1] // heads
    ep_count = lax.axis_size("ep")
    tp_count = lax.axis_size("tp")
    groups = ep_count // heads
    share = span // groups
    place = (lax.axis_index("ep") % groups).astype(jnp.int32).reshape(1)

    def spread(array):
        return jnp.broadcast_to(array[:, None], (heads, groups) + array.shape[1:]).reshape(
            (ep_count,) + array.shape[1:]
        )

    query_parts = (
        queries.reshape(groups, share, heads, size)
        .transpose(2, 0, 1, 3)
        .reshape(ep_count, share, size)
    )
    key_parts = spread(keys.reshape(span, heads, size).transpose(1, 0, 2))
    value_parts = spread(values.reshape(span, heads, size).transpose(1, 0, 2))
    bias_parts = key_bias.T.reshape(heads, span // size, size)
    bias_parts = spread(jnp.pad(bias_parts, ((0, 0), (0, BIAS_ROWS - span // size), (0, 0))))
    data = lax.all_to_all(
        jnp.concatenate([query_parts, key_parts, value_parts, bias_parts], axis=1),
        "ep",
        split_axis=0,
        concat_axis=0,
        tiled=True,
    )
    mixed_heads = attention(data, place, share, span)
    mixed_heads = lax.all_to_all(mixed_heads, "ep", split_axis=0, concat_axis=0, tiled=True)
    heads_out = (
        mixed_heads.reshape(heads, groups, share, size)
        .transpose(1, 2, 0, 3)
        .reshape(span, heads * size)
    )
    col_count = out_weight.shape[1] // tp_count
    weight_cols = lax.all_to_all(
        out_weight.reshape(-1, tp_count, col_count).transpose(1, 0, 2),
        "tp",
        split_axis=0,
        concat_axis=0,
        tiled=True,
    )
    heads_all = lax.all_gather(heads_out, "tp", axis=0)
    mixed_tokens = jnp.einsum(
        "trh,thd->rd", heads_all, weight_cols, preferred_element_type=jnp.float32
    ).astype(jnp.bfloat16)

    token_count = moe_input.shape[0]
    inputs = moe_input.astype(jnp.float32)
    normed = (
        inputs * lax.rsqrt(jnp.mean(inputs * inputs, axis=-1, keepdims=True) + EPS_NORM) * moe_gain
    ).astype(jnp.bfloat16)
    own_cols = lax.dynamic_slice_in_dim(normed, lax.axis_index("tp") * col_count, col_count, 1)
    shared_hidden = (
        jax.nn.silu(jnp.dot(normed, shared_gate, preferred_element_type=jnp.float32))
        * jnp.dot(normed, shared_up, preferred_element_type=jnp.float32)
    ).astype(jnp.bfloat16)
    local_experts = expert_gate.shape[0]
    expert_count = local_experts * ep_count
    topk = route_ids.shape[1]
    capacity = 3 * token_count * topk // (2 * expert_count)
    send_slots = expert_count * capacity
    onehot = route_ids[:, :, None] == jnp.arange(expert_count, dtype=jnp.int32)
    named = jnp.sum(onehot.astype(jnp.bfloat16), axis=1)
    row = jnp.arange(token_count)
    earlier = jnp.dot(
        (row[:, None] > row[None, :]).astype(jnp.bfloat16),
        named,
        preferred_element_type=jnp.float32,
    ).astype(jnp.int32)
    place_in = jnp.sum(jnp.where(onehot, earlier[:, None, :], 0), axis=2)
    slot_ids = route_ids * capacity + place_in
    matches = slot_ids[None] == jnp.arange(send_slots, dtype=jnp.int32)[:, None, None]
    dispatch = jnp.sum(matches.astype(jnp.bfloat16), axis=2)
    outgoing = jnp.dot(dispatch, own_cols, preferred_element_type=jnp.float32).astype(jnp.bfloat16)
    arrived = lax.all_to_all(outgoing, "ep", split_axis=0, concat_axis=0, tiled=True)
    piece = lax.all_gather(arrived, "tp", axis=1, tiled=True)
    width = piece.shape[1]
    grid = piece.reshape(ep_count, local_experts, capacity, width)
    gate_sum = jnp.einsum("secd,edf->secf", grid, expert_gate, preferred_element_type=jnp.float32)
    up_sum = jnp.einsum("secd,edf->secf", grid, expert_up, preferred_element_type=jnp.float32)
    expert_hidden = (jax.nn.silu(gate_sum) * up_sum).astype(jnp.bfloat16)
    routed = jnp.einsum(
        "secf,efd->dsec", expert_hidden, expert_down, preferred_element_type=jnp.float32
    ).reshape(tp_count * col_count, -1)
    common = jnp.einsum("tf,fd->dt", shared_hidden, shared_down, preferred_element_type=jnp.float32)
    expert_sum = lax.psum_scatter(
        jnp.concatenate([routed, common], axis=1).astype(jnp.bfloat16),
        "tp",
        scatter_dimension=0,
        tiled=True,
    )
    routed_sum = expert_sum[:, :send_slots]
    common_sum = expert_sum[:, send_slots:].astype(jnp.float32)
    returned = lax.all_to_all(routed_sum, "ep", split_axis=1, concat_axis=1, tiled=True)
    gates = route_scores / jnp.sum(route_scores, axis=-1, keepdims=True) * ROUTED_SCALE
    gates_high = gates.astype(jnp.bfloat16)
    gates_low = (gates - gates_high.astype(jnp.float32)).astype(jnp.bfloat16)

    def combined(part):
        table = jnp.sum(jnp.where(matches, part[None], jnp.bfloat16(0)), axis=2)
        return jnp.einsum("ds,st->td", returned, table, preferred_element_type=jnp.float32)

    expert_mix = (common_sum.T + combined(gates_high) + combined(gates_low)).astype(jnp.bfloat16)
    return (mixed_tokens, expert_mix)


def solution(mesh):
    return jax.shard_map(
        body,
        mesh=mesh,
        in_specs=(
            P("ep", "tp"),
            P("ep", "tp"),
            P("ep", "tp"),
            P("ep", "tp"),
            P("tp", None),
            P("ep", None),
            P(),
            P("ep", None),
            P("ep", None),
            P(None, "tp"),
            P(None, "tp"),
            P("tp", None),
            P("ep", None, "tp"),
            P("ep", None, "tp"),
            P("ep", "tp", None),
        ),
        out_specs=(P("ep", "tp"), P("ep", "tp")),
        check_vma=False,
    )
```

time: 472 us -> 214 us (0.45)
  other arithmetic: 149 us -> 10.1 us
  local copies, waits for them, and re-layouts: 85 us -> 20.9 us
  matrix products: 54.8 us -> 17.1 us
  Pallas kernels: 0 us -> 27.3 us
  waiting for transfers between devices: 97.3 us -> 73.5 us
  starting transfers between devices: 25.3 us -> 12.7 us
  loops' own time: 8.35 us -> 0 us
  blocking collectives: 31.9 us -> 37.3 us
    another operation x29 -> x0, other arithmetic: 110 us -> none
    all_to_all x1 -> x2, waiting for transfers between devices: 0.01 us -> 70.3 us  [the longest x1 46.6 us: body(): lax.all_to_all(jnp.concatenate([query_parts, key_parts, value_parts, bias...]
    reduce_scatter x1, waiting for transfers between devices: 44.3 us -> 0.02 us  [body(): lax.psum_scatter(jnp.concatenate([routed, common], axis=1).astype(jnp.bfl...]
    all_to_all x0 -> x2, blocking collectives: none -> 37.3 us  [the longest x1 19.2 us: body(): lax.all_to_all(outgoing, 'ep', split_axis=0, concat_axis=0, tiled=True)]
    ppermute x6 -> x0, waiting for transfers between devices: 37 us -> none  [partner_2(): lax.ppermute(array, axis, [(i, i ^ 1 << apart) for i in range(lax.axis_si...]
    dot_general x19 -> x4, matrix products: 42.8 us -> 6.46 us  [the longest x1 4.26 us: body(): jnp.einsum('trh,thd->rd', heads_all, weight_cols, preferred_element_type=...]
    another operation x35 -> x1, local copies, waits for them, and re-layouts: 34.2 us -> 0.99 us  [body(): heads_all = lax.all_gather(heads_out, 'tp', axis=0)]
    all_gather x1 -> x0, blocking collectives: 31.9 us -> none  [body(): lax.all_gather(own_piece[2], 'ep', axis=0, tiled=True)]
  transfers between devices with their start and end apart: 12 -> 6, of which waited for: 8 -> 3; matrix products, arithmetic and copies ran while one was open for 55% -> 17% of each run, Pallas kernels for 0% -> 13%
where the time goes in v1:
time: 214 us; the launch traced here: 213 us
  waiting for transfers between devices  73.5 us (34%)
  blocking collectives  37.3 us (17%)
  Pallas kernels  27.3 us (13%)
  local copies, waits for them, and re-layouts  20.9 us (10%)
  matrix products  17.1 us (8%)
  between operations  14 us (7%)
  starting transfers between devices  12.7 us (6%)
  other arithmetic  10.1 us (5%)
    all_to_all x1, waiting for transfers between devices, body(): lax.all_to_all(jnp.concatenate([query_parts, key_parts, value_parts, bias...  46.6 us
    pallas_call x1, Pallas kernels, attention(): pl.pallas_call(functools.partial(attention_kernel, share, span), grid=(bl...  27.3 us
    all_to_all x1, waiting for transfers between devices, body(): lax.all_to_all(out_weight.reshape(-1, tp_count, col_count).transpose(1, 0...  23.7 us
    all_to_all x1, blocking collectives, body(): lax.all_to_all(outgoing, 'ep', split_axis=0, concat_axis=0, tiled=True)  19.2 us
    all_to_all x1, blocking collectives, body(): lax.all_to_all(mixed_heads, 'ep', split_axis=0, concat_axis=0, tiled=True)  18 us
    all_to_all x1, starting transfers between devices, body(): lax.all_to_all(out_weight.reshape(-1, tp_count, col_count).transpose(1, 0...  4.57 us
    all_to_all x1, starting transfers between devices, body(): lax.all_to_all(jnp.concatenate([query_parts, key_parts, value_parts, bias...  4.39 us
  transfers between devices with their start and end apart: 6, of which 3 were waited for; matrix products, arithmetic and copies ran while one was open for 17% of the time, Pallas kernels for 13%

profile of v1, /device:TPU:0, one launch (start us, length us, event | category | flops | bytes accessed | tf_op | source)
XLA Modules:
  0.0 212.8 jit_solution(365857399884999296)
XLA Ops:
  7.2 0.0 copy-start
  7.2 0.0 copy-start.4
  7.2 0.0 copy-start.2
  7.2 0.0 all-gather.5.cloned.1.call-start
  7.2 0.8 fusion.40
  8.1 0.1 convolution_convert_fusion.3
  8.2 0.7 select_reduce_fusion
  8.9 0.7 multiply_add_fusion
  9.6 0.7 reduce_sum.79
  10.3 0.7 subtract_convert_fusion
  11.0 1.2 fusion.22
  12.2 1.2 fusion.24
  13.5 0.7 fusion.36
  14.2 0.2 convolution_convert_fusion.2
  14.5 19.2 %all_to_all.39 = bf16[8,48,512]{2,1,0:T(8,128)(2,1)} all-to-all(bf16[8,48,512]{2,1,0:T(8,128)(2,1)S(1)} %bitcast.93), channel_id=1, replica_groups=mesh['ep'=8,'tp'=4] {'ep'}, dimensions={0} | all-to-all | bytes 786432 | tf_op jit(solution)/shard_map/all_to_all | solution.py:199
  33.7 0.0 all-gather.5.cloned.1.call-update
  33.7 0.0 copy-done.4
  33.8 0.0 copy-done.2
  33.8 0.9 reshape.87
  34.7 1.1 copy.50
  35.8 2.0 reshape.85
  37.8 1.9 copy.49
  39.7 2.1 reshape.83
  41.8 0.0 copy-start.1
  41.8 1.2 copy.48
  43.0 0.1 broadcast_in_dim.33
  43.1 0.0 copy-done.1
  43.1 0.1 broadcast_in_dim.32
  43.3 1.6 pad_maximum_fusion
  44.9 4.4 %all-to-all-start = ((bf16[8,1296,128]{2,1,0:T(8,128)(2,1)}), bf16[8,1296,128]{2,1,0:T(8,128)(2,1)}, u32[]{:S(2)}, u32[]{:S(2)}) async-start(bf16[8,1296,128]{2,1,0:T(8,128)(2,1)} %pad_maximum_fusion), calls=%async_computation | async-start | bytes 5308416 | tf_op jit(solution)/shard_map/all_to_all | solution.py:144
  49.3 0.0 reduce-scatter.2.cloned.1.call-start
  49.4 2.0 fusion.43
  51.4 3.1 %fusion.1 = bf16[2048,128]{0,1:T(8,128)(2,1)S(1)} fusion(bf16[512,2048]{1,0:T(8,128)(2,1)} %param.26, bf16[128,2048]{1,0:T(8,128)(2,1)S(1)} %fusion.24, bf16[2048,512]{1,0:T(8,128)(2,1)} %param.25, f32[128,512]{1,0:T(8,128)S(1)} %fusion.43), kind=kOutput, calls=%fused_computation.4 | convolution fusion | flops 537526272 | bytes 5505024 | tf_op jit(solution)/shard_map/tf,fd->dt/dot_general | solution.py:209
  54.5 0.0 all-gather.5.cloned.1.call-done
  54.5 0.0 copy-start.5
  54.5 0.0 copy-start.6
  54.6 3.2 %fusion.8 = f32[8,1,48,512]{3,2,0,1:T(8,128)S(1)} fusion(bf16[8,48,2048]{2,1,0:T(8,128)(2,1)} %bitcast.96, bf16[1,2048,512]{2,1,0:T(8,128)(2,1)} %param.27), kind=kOutput, calls=%fused_computation.15 | convolution fusion | flops 805306368 | bytes 4456448 | tf_op jit(solution)/shard_map/secd,edf->secf/dot_general | solution.py:203
  57.7 0.0 copy-done.5
  57.8 0.0 copy-done.6
  57.8 1.0 fusion.17
  58.8 0.0 copy-done
  58.8 1.0 fusion
  59.8 1.6 pad_maximum_fusion.1
  61.4 0.0 reduce-scatter.2.cloned.1.call-update
  61.4 0.0 all-gather.3.cloned.1.call-start
  61.5 46.6 %all-to-all-done.data_ref = bf16[8,1296,128]{2,1,0:T(8,128)(2,1)} async-done(((bf16[8,1296,128]{2,1,0:T(8,128)(2,1)}), bf16[8,1296,128]{2,1,0:T(8,128)(2,1)}, u32[]{:S(2)}, u32[]{:S(2)}) %all-to-all-start) | async-done | bytes 2654240 | tf_op jit(solution)/shard_map/all_to_all | solution.py:144
  108.1 27.3 %stick.1 = bf16[8,256,128]{2,1,0:T(8,128)(2,1)S(1)} custom-call(s32[1]{0:T(128)} %bitcast.place_ref, bf16[8,1296,128]{2,1,0:T(8,128)(2,1)} %all-to-all-done.data_ref, bf16[256,256]{1,0:T(8,128)(2,1)S(1)} %fusion.33.tri_ref), custom_call_target="tpu_custom_call" | custom-call | flops 4831838208 | bytes 2654208 | tf_op jit(solution)/shard_map/stick/pallas_call | solution.py:82
  135.4 18.0 %all_to_all.40 = bf16[8,256,128]{2,1,0:T(8,128)(2,1)S(1)} all-to-all(bf16[8,256,128]{2,1,0:T(8,128)(2,1)S(1)} %stick.1), channel_id=1, replica_groups=mesh['ep'=8,'tp'=4] {'ep'}, dimensions={0} | all-to-all | bytes 1048576 | tf_op jit(solution)/shard_map/all_to_all | solution.py:152
  153.5 0.4 copy.51
  153.9 1.0 all_gather_reshape.3
  154.9 0.0 all-gather.3.cloned.1.call-update
  154.9 0.0 reduce-scatter.2.cloned.1.call-done
  154.9 1.8 slice.9
  156.7 3.6 %all-to-all-start.4 = ((bf16[512,8,48]{0,2,1:T(8,128)(2,1)}), bf16[512,8,48]{0,2,1:T(8,128)(2,1)S(1)}, u32[]{:S(2)}, u32[]{:S(2)}) async-start(bf16[512,8,48]{0,2,1:T(8,128)(2,1)} %bitcast.34), calls=%async_computation.5 | async-start | bytes 786432 | tf_op jit(solution)/shard_map/all_to_all | solution.py:218
  160.3 4.0 %copy.52 = bf16[512,2048]{0,1:T(8,128)(2,1)} copy(bf16[512,2048]{1,0:T(8,128)(2,1)} %param.19) | data formatting | bytes 4194304 | tf_op args[4]
  164.4 4.2 %copy.53 = bf16[512,4,512]{2,0,1:T(8,128)(2,1)} copy(bf16[512,4,512]{0,2,1:T(8,128)(2,1)} %bitcast.83) | data formatting | bytes 4194304 | tf_op jit(solution)/shard_map/reshape | solution.py:160
  168.5 3.2 %all-to-all-done.4 = bf16[512,8,48]{0,2,1:T(8,128)(2,1)S(1)} async-done(((bf16[512,8,48]{0,2,1:T(8,128)(2,1)}), bf16[512,8,48]{0,2,1:T(8,128)(2,1)S(1)}, u32[]{:S(2)}, u32[]{:S(2)}) %all-to-all-start.4) | async-done | bytes 393248 | tf_op jit(solution)/shard_map/all_to_all | solution.py:218
  171.7 0.0 copy-start.3
  171.7 4.6 %all-to-all-start.2 = ((bf16[4,512,512]{2,1,0:T(8,128)(2,1)}), bf16[4,512,512]{2,1,0:T(8,128)(2,1)}, u32[]{:S(2)}, u32[]{:S(2)}) async-start(bf16[4,512,512]{2,1,0:T(8,128)(2,1)} %bitcast.82), calls=%async_computation.2 | async-start | bytes 4194304 | tf_op jit(solution)/shard_map/all_to_all | solution.py:159
  176.3 0.0 copy-done.3
  176.3 1.2 convolution_add_fusion.1
  177.4 0.9 fusion.21
  178.3 23.7 %all-to-all-done.2 = bf16[4,512,512]{2,1,0:T(8,128)(2,1)} async-done(((bf16[4,512,512]{2,1,0:T(8,128)(2,1)}), bf16[4,512,512]{2,1,0:T(8,128)(2,1)}, u32[]{:S(2)}, u32[]{:S(2)}) %all-to-all-start.2) | async-done | bytes 2097184 | tf_op jit(solution)/shard_map/all_to_all | solution.py:159
  202.0 4.3 %fusion.7 = bf16[512,512]{1,0:T(8,128)(2,1)} fusion(bf16[4,512,512]{2,1,0:T(8,128)(2,1)} %all-gather.3.cloned.1.call-done, bf16[4,512,512]{2,1,0:T(8,128)(2,1)} %all-to-all-done.2), kind=kOutput, calls=%fused_computation.14 | convolution fusion | flops 1074003968 | bytes 4718592 | tf_op jit(solution)/shard_map/trh,thd->rd/dot_general | solution.py:167
  (6 shorter events, 0.1 us)
Async XLA Ops:
  7.2 51.6 %copy-start = (bf16[1,512,2048]{2,1,0:T(8,128)(2,1)S(1)}, bf16[1,512,2048]{2,1,0:T(8,128)(2,1)}, u32[]{:S(2)}) copy-start(bf16[1,512,2048]{2,1,0:T(8,128)(2,1)} %param.29) | copy-start | bytes 6291460
  7.2 26.6 %copy-start.4 = (bf16[512,4]{0,1:T(4,128)(2,1)S(1)}, bf16[512,4]{0,1:T(4,128)(2,1)}, u32[]{:S(2)}) copy-start(bf16[512,4]{0,1:T(4,128)(2,1)} %param.18) | copy-start | bytes 12292
  7.2 26.6 %copy-start.2 = (bf16[512,512]{1,0:T(8,128)(2,1)S(1)}, bf16[512,512]{1,0:T(8,128)(2,1)}, u32[]{:S(2)}) copy-start(bf16[512,512]{1,0:T(8,128)(2,1)} %param.17) | copy-start | bytes 1572868
  7.2 47.3 %all-gather.5.cloned.1.call-start = ((), (), s32[]{:S(2)}) async-start(), calls=%async_computation.7 | async-start | bytes 1966080 | tf_op jit(solution)/shard_map/all_gather | solution.py:200
  41.8 1.4 copy-start.1
  44.9 63.2 %all-to-all-start = ((bf16[8,1296,128]{2,1,0:T(8,128)(2,1)}), bf16[8,1296,128]{2,1,0:T(8,128)(2,1)}, u32[]{:S(2)}, u32[]{:S(2)}) async-start(bf16[8,1296,128]{2,1,0:T(8,128)(2,1)} %pad_maximum_fusion), calls=%async_computation | async-start | bytes 5308416 | tf_op jit(solution)/shard_map/all_to_all | solution.py:144
  49.3 105.6 %reduce-scatter.2.cloned.1.call-start = ((), (), s32[]{:S(2)}) async-start(), calls=%async_computation.8 | async-start | bytes 2621440 | tf_op jit(solution)/shard_map/reduce_scatter | solution.py:210
  54.5 3.2 %copy-start.5 = (bf16[1,2048,512]{2,1,0:T(8,128)(2,1)S(1)}, bf16[1,2048,512]{2,1,0:T(8,128)(2,1)}, u32[]{:S(2)}) copy-start(bf16[1,2048,512]{2,1,0:T(8,128)(2,1)} %param.28) | copy-start | bytes 6291460
  54.5 3.2 %copy-start.6 = (bf16[384,2048]{1,0:T(8,128)(2,1)S(1)}, bf16[384,2048]{1,0:T(8,128)(2,1)}, u32[]{:S(2)}) copy-start(bf16[384,2048]{1,0:T(8,128)(2,1)} %all-gather.5.cloned.1.call-done) | copy-start | bytes 4718596
  61.4 140.5 %all-gather.3.cloned.1.call-start = ((), (), s32[]{:S(2)}) async-start(), calls=%async_computation.6 | async-start | bytes 2621440 | tf_op jit(solution)/shard_map/all_gather | solution.py:166
  156.7 15.0 %all-to-all-start.4 = ((bf16[512,8,48]{0,2,1:T(8,128)(2,1)}), bf16[512,8,48]{0,2,1:T(8,128)(2,1)S(1)}, u32[]{:S(2)}, u32[]{:S(2)}) async-start(bf16[512,8,48]{0,2,1:T(8,128)(2,1)} %bitcast.34), calls=%async_computation.5 | async-start | bytes 786432 | tf_op jit(solution)/shard_map/all_to_all | solution.py:218
  171.7 4.6 %copy-start.3 = (bf16[384,128]{1,0:T(8,128)(2,1)S(1)}, bf16[384,128]{1,0:T(8,128)(2,1)}, u32[]{:S(2)}) copy-start(bf16[384,128]{1,0:T(8,128)(2,1)} %get-tuple-element.3) | copy-start | bytes 294916
  171.7 30.3 %all-to-all-start.2 = ((bf16[4,512,512]{2,1,0:T(8,128)(2,1)}), bf16[4,512,512]{2,1,0:T(8,128)(2,1)}, u32[]{:S(2)}, u32[]{:S(2)}) async-start(bf16[4,512,512]{2,1,0:T(8,128)(2,1)} %bitcast.82), calls=%async_computation.2 | async-start | bytes 4194304 | tf_op jit(solution)/shard_map/all_to_all | solution.py:159
Sparse Core Ops, SparseCore 0:
  33.9 18.3 all-gather.4
  61.6 32.3 reduce-scatter.1
  155.0 21.6 all-gather.2

commit v2 on v1

--- a/solution.py
+++ b/solution.py
@@ -11,28 +11,26 @@
 ROUTED_SCALE = 2.5
 LOG2E = 1.4426950408889634
 BIAS_ROWS = 16
-
-
-def attention_kernel(share, span, place_ref, data_ref, tri_ref, out_ref):
+MESH = pl.DeviceIdType.MESH
+
+
+def attention_kernel(place_ref, query_ref, key_ref, value_ref, bias_ref, tri_ref, out_ref):
     block = pl.program_id(0)
+    share, size = query_ref.shape[1:]
+    span = key_ref.shape[1]
     offset = place_ref[0] * share
     width = tri_ref.shape[0]
-    size = out_ref.shape[2]
-    query = data_ref[block, pl.ds(0, share), :]
+    query = query_ref[block]
     scale = size ** (-0.5) * LOG2E
 
     def unit(key_block, carry, masked):
         total, passed = carry
-        key = data_ref[key_block, pl.ds(share, span), :]
-        value = data_ref[key_block, pl.ds(share + span, span), :]
-        bias = data_ref[key_block, pl.ds(share + 2 * span, BIAS_ROWS), :].astype(jnp.float32)
-        bias = bias * LOG2E
+        key = key_ref[key_block]
+        value = value_ref[key_block]
+        bias = bias_ref[key_block].astype(jnp.float32) * LOG2E
         for start in range(span - width, -1, -width):
             row = jnp.concatenate(
-                [
-                    bias[i : i + 1, :]
-                    for i in range(start // size, (start + width) // size)
-                ],
+                [bias[i : i + 1, :] for i in range(start // size, (start + width) // size)],
                 axis=1,
             )
             logit = (
@@ -73,32 +71,401 @@
     out_ref[0] = carry[0].astype(out_ref.dtype)
 
 
-def attention(data, place, share, span):
-    blocks, _, size = data.shape
+def attention(query, key, value, bias, place):
+    blocks, share, size = query.shape
+    span = key.shape[1]
     width = min(256, span)
     index = jnp.arange(width)
     tri = (index[:, None] > index[None, :]).astype(jnp.bfloat16)
     work = blocks * (blocks + 1) // 2 * share * span
+    whole = pl.BlockSpec(memory_space=pltpu.VMEM)
     return pl.pallas_call(
-        functools.partial(attention_kernel, share, span),
+        attention_kernel,
         grid=(blocks,),
-        in_specs=[
-            pl.BlockSpec(memory_space=pltpu.SMEM),
-            pl.BlockSpec(memory_space=pltpu.VMEM),
-            pl.BlockSpec(memory_space=pltpu.VMEM),
-        ],
+        in_specs=[pl.BlockSpec(memory_space=pltpu.SMEM)] + [whole] * 5,
         out_specs=pl.BlockSpec((1, share, size), lambda i: (i, 0, 0)),
         out_shape=jax.ShapeDtypeStruct((blocks, share, size), jnp.bfloat16),
         cost_estimate=pl.CostEstimate(
             flops=work * (4 * size + 2 * width),
-            bytes_accessed=data.size * 2,
+            bytes_accessed=key.size * 5,
             transcendentals=3 * work,
         ),
         compiler_params=pltpu.CompilerParams(
             dimension_semantics=("arbitrary",), vmem_limit_bytes=40 * 1024 * 1024
         ),
         name="stick",
-    )(place, data, tri)
+    )(place, query, key, value, bias, tri)
+
+
+def columns(index, width):
+    return pl.ds(pl.multiple_of(index * width, width), width)
+
+
+def meet(ep_count, tp_count):
+    own_ep, own_tp = lax.axis_index("ep"), lax.axis_index("tp")
+    barrier = pltpu.get_barrier_semaphore()
+    for i in range(1, ep_count):
+        pl.semaphore_signal(
+            barrier, inc=1, device_id={"ep": lax.rem(own_ep + i, ep_count)}, device_id_type=MESH
+        )
+    for i in range(1, tp_count):
+        pl.semaphore_signal(
+            barrier, inc=1, device_id={"tp": lax.rem(own_tp + i, tp_count)}, device_id_type=MESH
+        )
+    pl.semaphore_wait(barrier, ep_count + tp_count - 2)
+
+
+def exchange_kernel(
+    counts,
+    query_ref,
+    key_ref,
+    value_ref,
+    bias_ref,
+    rows_ref,
+    weight_ref,
+    query_out,
+    key_out,
+    value_out,
+    bias_out,
+    rows_out,
+    weight_out,
+    local_sem,
+    query_send,
+    query_recv,
+    part_send,
+    part_recv,
+    rows_send,
+    rows_recv,
+    relay_send,
+    relay_recv,
+    weight_send,
+    weight_recv,
+):
+    ep_count, tp_count, heads = counts
+    groups = ep_count // heads
+    share, size = query_out.shape[1:]
+    depth = weight_ref.shape[0]
+    col_count = weight_out.shape[1]
+    own, own_tp = lax.axis_index("ep"), lax.axis_index("tp")
+    own_head, own_group = own // groups, lax.rem(own, groups)
+    rows_own = rows_out.at[:, :, columns(own_tp, col_count)]
+
+    def query_part(device):
+        return query_ref.at[columns(lax.rem(device, groups), share), columns(device // groups, size)]
+
+    def part(kind, head):
+        if kind == 2:
+            return bias_ref.at[head]
+        return (key_ref, value_ref)[kind].at[:, columns(head, size)]
+
+    part_outs = (key_out, value_out, bias_out)
+
+    def remote(source, target, send, recv, axis, device):
+        return pltpu.make_async_remote_copy(
+            src_ref=source,
+            dst_ref=target,
+            send_sem=send,
+            recv_sem=recv,
+            device_id={axis: device},
+            device_id_type=MESH,
+        )
+
+    meet(ep_count, tp_count)
+    sent = []
+
+    def start(copy):
+        copy.start()
+        sent.append(copy)
+
+    local = [
+        pltpu.make_async_copy(rows_ref.at[own], rows_out.at[own, :, columns(own_tp, col_count)], local_sem.at[0]),
+        pltpu.make_async_copy(query_part(own), query_out.at[own], local_sem.at[1]),
+        pltpu.make_async_copy(
+            weight_ref.at[:, columns(own_tp, col_count)],
+            weight_out.at[columns(own_tp, depth), :],
+            local_sem.at[2],
+        ),
+    ] + [
+        pltpu.make_async_copy(part(kind, own_head), part_outs[kind].at[own], local_sem.at[3 + kind])
+        for kind in range(3)
+    ]
+    for copy in local:
+        copy.start()
+    for i in range(1, ep_count):
+        other = lax.rem(own + i, ep_count)
+        start(
+            remote(
+                rows_ref.at[other],
+                rows_out.at[own, :, columns(own_tp, col_count)],
+                rows_send.at[other],
+                rows_recv.at[own],
+                "ep",
+                other,
+            )
+        )
+    for step in range(1, groups):
+        group = lax.rem(own_group + step, groups)
+        other = own_head * groups + group
+        for kind in range(3):
+            start(
+                remote(
+                    part(kind, own_head),
+                    part_outs[kind].at[own],
+                    part_send.at[kind, other],
+                    part_recv.at[kind, own],
+                    "ep",
+                    other,
+                )
+            )
+    for i in range(1, heads):
+        head = lax.rem(own_head + i, heads)
+        other = head * groups + own_group
+        for kind in range(3):
+            start(
+                remote(
+                    part(kind, head),
+                    part_outs[kind].at[own],
+                    part_send.at[kind, other],
+                    part_recv.at[kind, own],
+                    "ep",
+                    other,
+                )
+            )
+    for i in range(1, ep_count):
+        other = lax.rem(own + i, ep_count)
+        start(
+            remote(
+                query_part(other),
+                query_out.at[own],
+                query_send.at[other],
+                query_recv.at[own],
+                "ep",
+                other,
+            )
+        )
+    for i in range(1, ep_count):
+        other = lax.rem(own + i, ep_count)
+        remote(
+            rows_ref.at[other],
+            rows_out.at[other, :, columns(own_tp, col_count)],
+            rows_send.at[other],
+            rows_recv.at[other],
+            "ep",
+            other,
+        ).wait_recv()
+    local[0].wait()
+    for i in range(1, tp_count):
+        other = lax.rem(own_tp + i, tp_count)
+        start(remote(rows_own, rows_own, relay_send.at[other], relay_recv.at[own_tp], "tp", other))
+    for i in range(1, tp_count):
+        other = lax.rem(own_tp + i, tp_count)
+        start(
+            remote(
+                weight_ref.at[:, columns(other, col_count)],
+                weight_out.at[columns(own_tp, depth), :],
+                weight_send.at[other],
+                weight_recv.at[own_tp],
+                "tp",
+                other,
+            )
+        )
+
+    def part_arrival(kind, source):
+        target = part_outs[kind].at[source]
+        remote(
+            target, target, part_send.at[kind, source], part_recv.at[kind, source], "ep", source
+        ).wait_recv()
+
+    for i in range(1, heads):
+        source = lax.rem(own_head + heads - i, heads) * groups + own_group
+        for kind in range(3):
+            part_arrival(kind, source)
+            for step in range(1, groups):
+                group = lax.rem(own_group + step, groups)
+                target = part_outs[kind].at[source]
+                start(
+                    remote(
+                        target,
+                        target,
+                        part_send.at[kind, source - own_group + group],
+                        part_recv.at[kind, source],
+                        "ep",
+                        own_head * groups + group,
+                    )
+                )
+    for i in range(heads):
+        for step in range(1, groups):
+            group = lax.rem(own_group + step, groups)
+            source = lax.rem(own_head + heads - i, heads) * groups + group
+            for kind in range(3):
+                part_arrival(kind, source)
+    for i in range(1, ep_count):
+        other = lax.rem(own + i, ep_count)
+        remote(
+            query_part(other),
+            query_out.at[other],
+            query_send.at[other],
+            query_recv.at[other],
+            "ep",
+            other,
+        ).wait_recv()
+    for i in range(1, tp_count):
+        other = lax.rem(own_tp + i, tp_count)
+        arrived = rows_out.at[:, :, columns(other, col_count)]
+        remote(
+            arrived, arrived, relay_send.at[other], relay_recv.at[other], "tp", other
+        ).wait_recv()
+        target = weight_out.at[columns(other, depth), :]
+        remote(
+            target, target, weight_send.at[other], weight_recv.at[other], "tp", other
+        ).wait_recv()
+    for copy in sent:
+        copy.wait_send()
+    for copy in local[1:]:
+        copy.wait()
+
+
+def exchange(queries, keys, values, bias, rows, weight, counts):
+    ep_count, tp_count, heads = counts
+    span = queries.shape[0]
+    size = queries.shape[1] // heads
+    share = span * heads // ep_count
+    depth, features = weight.shape
+    whole = pl.BlockSpec(memory_space=pltpu.VMEM)
+    free = pl.BlockSpec(memory_space=pl.ANY)
+    dma = pltpu.SemaphoreType.DMA
+    kind = jnp.bfloat16
+    return pl.pallas_call(
+        functools.partial(exchange_kernel, counts),
+        in_specs=[whole] * 6,
+        out_specs=[free] * 6,
+        out_shape=[
+            jax.ShapeDtypeStruct((ep_count, share, size), kind),
+            jax.ShapeDtypeStruct((ep_count, span, size), kind),
+            jax.ShapeDtypeStruct((ep_count, span, size), kind),
+            jax.ShapeDtypeStruct((ep_count,) + bias.shape[1:], kind),
+            jax.ShapeDtypeStruct((ep_count, rows.shape[1], features), kind),
+            jax.ShapeDtypeStruct((depth * tp_count, features // tp_count), kind),
+        ],
+        scratch_shapes=[
+            dma((6,)),
+            dma((ep_count,)),
+            dma((ep_count,)),
+            dma((3, ep_count)),
+            dma((3, ep_count)),
+            dma((ep_count,)),
+            dma((ep_count,)),
+            dma((tp_count,)),
+            dma((tp_count,)),
+            dma((tp_count,)),
+            dma((tp_count,)),
+        ],
+        compiler_params=pltpu.CompilerParams(
+            collective_id=0, has_side_effects=True, vmem_limit_bytes=40 * 1024 * 1024
+        ),
+        name="exchange",
+    )(queries, keys, values, bias, rows, weight)
+
+
+def gather_kernel(counts, part_ref, out_ref, local_sem, send_sem, recv_sem, relay_send, relay_recv):
+    ep_count, tp_count, heads = counts
+    groups = ep_count // heads
+    share, size = part_ref.shape[1:]
+    own, own_tp = lax.axis_index("ep"), lax.axis_index("tp")
+
+    def place_of(source, slot):
+        return out_ref.at[
+            columns(lax.rem(source, groups), share), columns(slot * heads + source // groups, size)
+        ]
+
+    def remote(source, target, send, recv, axis, device):
+        return pltpu.make_async_remote_copy(
+            src_ref=source,
+            dst_ref=target,
+            send_sem=send,
+            recv_sem=recv,
+            device_id={axis: device},
+            device_id_type=MESH,
+        )
+
+    meet(ep_count, tp_count)
+    local = pltpu.make_async_copy(part_ref.at[own], place_of(own, own_tp), local_sem.at[0])
+    local.start()
+    sent = []
+    for i in range(1, ep_count):
+        other = lax.rem(own + i, ep_count)
+        copy = remote(
+            part_ref.at[other],
+            place_of(own, own_tp),
+            send_sem.at[other],
+            recv_sem.at[own],
+            "ep",
+            other,
+        )
+        copy.start()
+        sent.append(copy)
+    for i in range(ep_count):
+        source = lax.rem(own + ep_count - i, ep_count)
+        piece = place_of(source, own_tp)
+        if i == 0:
+            local.wait()
+        else:
+            remote(
+                piece, piece, send_sem.at[source], recv_sem.at[source], "ep", source
+            ).wait_recv()
+        for j in range(1, tp_count):
+            other = lax.rem(own_tp + j, tp_count)
+            copy = remote(
+                piece,
+                piece,
+                relay_send.at[source, other],
+                relay_recv.at[source, own_tp],
+                "tp",
+                other,
+            )
+            copy.start()
+            sent.append(copy)
+    for i in range(ep_count):
+        source = lax.rem(own + ep_count - i, ep_count)
+        for j in range(1, tp_count):
+            other = lax.rem(own_tp + j, tp_count)
+            piece = place_of(source, other)
+            remote(
+                piece,
+                piece,
+                relay_send.at[source, other],
+                relay_recv.at[source, other],
+                "tp",
+                other,
+            ).wait_recv()
+    for copy in sent:
+        copy.wait_send()
+
+
+def gather(parts, counts):
+    ep_count, tp_count, heads = counts
+    _, share, size = parts.shape
+    dma = pltpu.SemaphoreType.DMA
+    return pl.pallas_call(
+        functools.partial(gather_kernel, counts),
+        in_specs=[pl.BlockSpec(memory_space=pltpu.VMEM)],
+        out_specs=pl.BlockSpec(memory_space=pl.ANY),
+        out_shape=jax.ShapeDtypeStruct(
+            (share * ep_count // heads, tp_count * heads * size), jnp.bfloat16
+        ),
+        scratch_shapes=[
+            dma((1,)),
+            dma((ep_count,)),
+            dma((ep_count,)),
+            dma((ep_count, tp_count)),
+            dma((ep_count, tp_count)),
+        ],
+        compiler_params=pltpu.CompilerParams(collective_id=1, has_side_effects=True),
+        cost_estimate=pl.CostEstimate(
+            flops=0, bytes_accessed=parts.size * 100, transcendentals=0
+        ),
+        name="gather",
+    )(parts)
 
 
 def body(
@@ -127,46 +494,10 @@
     share = span // groups
     place = (lax.axis_index("ep") % groups).astype(jnp.int32).reshape(1)
 
-    def spread(array):
-        return jnp.broadcast_to(array[:, None], (heads, groups) + array.shape[1:]).reshape(
-            (ep_count,) + array.shape[1:]
-        )
-
-    query_parts = (
-        queries.reshape(groups, share, heads, size)
-        .transpose(2, 0, 1, 3)
-        .reshape(ep_count, share, size)
-    )
-    key_parts = spread(keys.reshape(span, heads, size).transpose(1, 0, 2))
-    value_parts = spread(values.reshape(span, heads, size).transpose(1, 0, 2))
+    counts = (ep_count, tp_count, heads)
+    col_count = out_weight.shape[1] // tp_count
     bias_parts = key_bias.T.reshape(heads, span // size, size)
-    bias_parts = spread(jnp.pad(bias_parts, ((0, 0), (0, BIAS_ROWS - span // size), (0, 0))))
-    data = lax.all_to_all(
-        jnp.concatenate([query_parts, key_parts, value_parts, bias_parts], axis=1),
-        "ep",
-        split_axis=0,
-        concat_axis=0,
-        tiled=True,
-    )
-    mixed_heads = attention(data, place, share, span)
-    mixed_heads = lax.all_to_all(mixed_heads, "ep", split_axis=0, concat_axis=0, tiled=True)
-    heads_out = (
-        mixed_heads.reshape(heads, groups, share, size)
-        .transpose(1, 2, 0, 3)
-        .reshape(span, heads * size)
-    )
-    col_count = out_weight.shape[1] // tp_count
-    weight_cols = lax.all_to_all(
-        out_weight.reshape(-1, tp_count, col_count).transpose(1, 0, 2),
-        "tp",
-        split_axis=0,
-        concat_axis=0,
-        tiled=True,
-    )
-    heads_all = lax.all_gather(heads_out, "tp", axis=0)
-    mixed_tokens = jnp.einsum(
-        "trh,thd->rd", heads_all, weight_cols, preferred_element_type=jnp.float32
-    ).astype(jnp.bfloat16)
+    bias_parts = jnp.pad(bias_parts, ((0, 0), (0, BIAS_ROWS - span // size), (0, 0)))
 
     token_count = moe_input.shape[0]
     inputs = moe_input.astype(jnp.float32)
@@ -196,10 +527,16 @@
     matches = slot_ids[None] == jnp.arange(send_slots, dtype=jnp.int32)[:, None, None]
     dispatch = jnp.sum(matches.astype(jnp.bfloat16), axis=2)
     outgoing = jnp.dot(dispatch, own_cols, preferred_element_type=jnp.float32).astype(jnp.bfloat16)
-    arrived = lax.all_to_all(outgoing, "ep", split_axis=0, concat_axis=0, tiled=True)
-    piece = lax.all_gather(arrived, "tp", axis=1, tiled=True)
-    width = piece.shape[1]
-    grid = piece.reshape(ep_count, local_experts, capacity, width)
+    query_all, key_all, value_all, bias_all, grid, weight_cols = exchange(
+        queries,
+        keys,
+        values,
+        bias_parts,
+        outgoing.reshape(ep_count, local_experts * capacity, col_count),
+        out_weight,
+        counts,
+    )
+    grid = grid.reshape(ep_count, local_experts, capacity, -1)
     gate_sum = jnp.einsum("secd,edf->secf", grid, expert_gate, preferred_element_type=jnp.float32)
     up_sum = jnp.einsum("secd,edf->secf", grid, expert_up, preferred_element_type=jnp.float32)
     expert_hidden = (jax.nn.silu(gate_sum) * up_sum).astype(jnp.bfloat16)
@@ -207,8 +544,15 @@
         "secf,efd->dsec", expert_hidden, expert_down, preferred_element_type=jnp.float32
     ).reshape(tp_count * col_count, -1)
     common = jnp.einsum("tf,fd->dt", shared_hidden, shared_down, preferred_element_type=jnp.float32)
+    partial = jnp.concatenate([routed, common], axis=1).astype(jnp.bfloat16)
+    partial, query_all = lax.optimization_barrier((partial, query_all))
+    mixed_heads = attention(query_all, key_all, value_all, bias_all, place)
+    heads_all = gather(mixed_heads, counts)
+    mixed_tokens = jnp.dot(heads_all, weight_cols, preferred_element_type=jnp.float32).astype(
+        jnp.bfloat16
+    )
     expert_sum = lax.psum_scatter(
-        jnp.concatenate([routed, common], axis=1).astype(jnp.bfloat16),
+        partial,
         "tp",
         scatter_dimension=0,
         tiled=True,

time: 214 us -> 210 us (0.981)
  Pallas kernels: 27.3 us -> 108 us
  blocking collectives: 37.3 us -> 0 us
  waiting for transfers between devices: 73.5 us -> 46 us
  local copies, waits for them, and re-layouts: 20.9 us -> 7.5 us
  starting transfers between devices: 12.7 us -> 5.53 us
    pallas_call x1 -> x3, Pallas kernels: 27.3 us -> 108 us  [the longest x1 51.8 us: exchange(): pl.pallas_call(functools.partial(exchange_kernel, counts), in_specs=[whol...]
    all_to_all x2 -> x0, waiting for transfers between devices: 70.3 us -> none  [the longest x1 46.6 us: body(): lax.all_to_all(jnp.concatenate([query_parts, key_parts, value_parts, bias...]
    reduce_scatter x1, waiting for transfers between devices: 0.02 us -> 46 us  [body(): lax.psum_scatter(partial, 'tp', scatter_dimension=0, tiled=True)]
    all_to_all x2 -> x0, blocking collectives: 37.3 us -> none  [the longest x1 19.2 us: body(): lax.all_to_all(outgoing, 'ep', split_axis=0, concat_axis=0, tiled=True)]
    reshape x5 -> x0, local copies, waits for them, and re-layouts: 10.3 us -> none  [the longest x1 4.15 us: body(): out_weight.reshape(-1, tp_count, col_count).transpose(1, 0, 2)]
    all_to_all x2 -> x0, starting transfers between devices: 8.96 us -> none  [the longest x1 4.57 us: body(): lax.all_to_all(out_weight.reshape(-1, tp_count, col_count).transpose(1, 0...]
    transpose x3 -> x0, local copies, waits for them, and re-layouts: 3.43 us -> none  [the longest x1 1.92 us: body(): key_parts = spread(keys.reshape(span, heads, size).transpose(1, 0, 2))]
    all_to_all x1, waiting for transfers between devices: 3.16 us -> 0.01 us  [body(): lax.all_to_all(routed_sum, 'ep', split_axis=1, concat_axis=1, tiled=True)]
  transfers between devices with their start and end apart: 6 -> 2, of which waited for: 3 -> 1; matrix products, arithmetic and copies ran while one was open for 17% -> 2% of each run, Pallas kernels for 13% -> 27%
where the time goes in v2:
time: 210 us
  Pallas kernels  108 us (51%)
  waiting for transfers between devices  46 us (22%)
  matrix products  18.3 us (9%)
  between operations  14.3 us (7%)
  other arithmetic  9.95 us (5%)
  local copies, waits for them, and re-layouts  7.5 us (4%)
  starting transfers between devices  5.53 us (3%)
    pallas_call x1, Pallas kernels, exchange(): pl.pallas_call(functools.partial(exchange_kernel, counts), in_specs=[whol...  51.8 us
    reduce_scatter x1, waiting for transfers between devices, body(): lax.psum_scatter(partial, 'tp', scatter_dimension=0, tiled=True)  46 us
    pallas_call x1, Pallas kernels, gather(): pl.pallas_call(functools.partial(gather_kernel, counts), in_specs=[pl.Blo...  30.7 us
    pallas_call x1, Pallas kernels, attention(): pl.pallas_call(attention_kernel, grid=(blocks,), in_specs=[pl.BlockSpec(m...  25.6 us
    all_to_all x1, starting transfers between devices, body(): lax.all_to_all(routed_sum, 'ep', split_axis=1, concat_axis=1, tiled=True)  5.49 us
    unnamed x30, local copies, waits for them, and re-layouts  5.02 us
    dot_general x1, matrix products, body(): jnp.dot(heads_all, weight_cols, preferred_element_type=jnp.float32)  4.3 us
  transfers between devices with their start and end apart: 2, of which 1 were waited for; matrix products, arithmetic and copies ran while one was open for 2% of the time, Pallas kernels for 27%

profile of v2, /device:TPU:0, one launch (start us, length us, event | category | flops | bytes accessed | tf_op | source)
XLA Modules:
  0.0 209.6 jit_solution(16910387101273928605)
XLA Ops:
  7.2 0.0 copy-start
  7.2 0.0 reduce-scatter.2.cloned.1.call-start
  7.2 0.8 reduce_sum.79
  8.1 0.7 subtract_convert_fusion
  8.8 0.7 fusion.39
  9.4 0.1 convolution_convert_fusion.4
  9.6 0.7 select_reduce_fusion
  10.3 0.7 multiply_add_fusion
  11.0 1.2 fusion.21
  12.2 0.7 reshape.52
  12.9 1.2 fusion.23
  14.2 0.0 copy-start.11
  14.2 0.0 copy-start.1
  14.2 0.0 copy-start.3
  14.2 0.0 copy-start.4
  14.2 0.0 copy-start.5
  14.2 2.3 %fusion.42 = f32[128,512]{1,0:T(8,128)S(1)} fusion(bf16[128,2048]{1,0:T(8,128)(2,1)S(1)} %fusion.23, bf16[2048,512]{1,0:T(8,128)(2,1)} %param.24), kind=kOutput, calls=%fused_computation.54 | convolution fusion | flops 268435456 | bytes 2883584 | tf_op jit(solution)/shard_map/dot_general | solution.py:509
  16.5 0.7 fusion.35
  17.2 0.2 convolution_convert_fusion.3
  17.5 0.0 copy-start.13
  17.5 0.0 copy-done.11
  17.5 0.0 copy-done.1
  17.5 0.0 copy-done.3
  17.5 0.0 copy-done.4
  17.5 0.0 copy-done.5
  17.5 51.8 %exchange.1 = (bf16[8,256,128]{2,1,0:T(8,128)(2,1)S(1)}, bf16[8,512,128]{2,1,0:T(8,128)(2,1)S(1)}, bf16[8,512,128]{2,1,0:T(8,128)(2,1)S(1)}, bf16[8,16,128]{2,1,...) custom-call(bf16[512,512]{1,0:T(8,128)(2,1)S(1)} %copy-done.3, ...), custom_call_target="tpu_custom_call" | custom-call | tf_op jit(solution)/shard_map/exchange/pallas_call | solution.py:338
  69.3 0.0 copy-start.6
  69.3 0.0 copy-start.7
  69.4 0.0 copy-start.9
  69.4 0.0 copy-done.13
  69.4 0.0 copy-start.14
  69.4 1.0 fusion.7
  70.4 0.3 copy-done.6
  70.7 0.3 copy-done.7
  71.0 0.2 copy-done.9
  71.2 1.1 copy-done.14
  72.3 1.0 fusion.16
  73.3 0.0 copy-done
  73.3 2.2 %fusion = bf16[2048,384]{0,1:T(8,128)(2,1)} fusion(bf16[384,512]{1,0:T(8,128)(2,1)S(1)} %bitcast.66, bf16[1,512,2048]{2,1,0:T(8,128)(2,1)S(1)} %copy-done), kind=kOutput, calls=%fused_computation.1 | convolution fusion | flops 806092800 | bytes 4063232 | tf_op jit(solution)/shard_map/secf,efd->dsec/dot_general | solution.py:543
  75.5 4.0 %fusion.1 = bf16[2048,128]{0,1:T(8,128)(2,1)} fusion(bf16[512,2048]{1,0:T(8,128)(2,1)} %param.26, bf16[128,2048]{1,0:T(8,128)(2,1)} %copy-done.11, bf16[2048,512]{1,0:T(8,128)(2,1)} %param.25, f32[128,512]{1,0:T(8,128)S(1)} %fusion.42), kind=kOutput, calls=%fused_computation.3 | convolution fusion | flops 537526272 | bytes 5505024 | tf_op jit(solution)/shard_map/tf,fd->dt/dot_general | solution.py:546
  79.5 3.1 %pad_maximum_fusion = bf16[2048,512]{0,1:T(8,128)(2,1)} fusion(bf16[2048,128]{0,1:T(8,128)(2,1)} %fusion.1, bf16[2048,384]{0,1:T(8,128)(2,1)} %fusion), kind=kLoop, calls=%fused_computation.4 | loop fusion | flops 4194304 | bytes 4194304 | tf_op jit(solution)/shard_map/concatenate | solution.py:547
  82.6 0.0 reduce-scatter.2.cloned.1.call-update
  82.7 46.0 %reduce-scatter.2.cloned.1.call-done = bf16[512,512]{0,1:T(8,128)(2,1)} async-done(((bf16[2048,512]{0,1:T(8,128)(2,1)}), bf16[512,512]{0,1:T(8,128)(2,1)}) %reduce-scatter.2.cloned.1.call-update) | async-done | bytes 524304 | tf_op jit(solution)/shard_map/reduce_scatter | solution.py:554
  128.7 1.8 slice.9
  130.5 5.5 %all-to-all-start = ((bf16[512,8,48]{0,2,1:T(8,128)(2,1)}), bf16[512,8,48]{0,2,1:T(8,128)(2,1)}, u32[]{:S(2)}, u32[]{:S(2)}) async-start(bf16[512,8,48]{0,2,1:T(8,128)(2,1)} %bitcast.64), calls=%async_computation.1 | async-start | bytes 786432 | tf_op jit(solution)/shard_map/all_to_all | solution.py:562
  136.0 0.0 copy-start.8
  136.0 1.2 copy-done.8
  137.2 0.0 copy-start.10
  137.2 1.0 copy-done.10
  138.2 25.6 %stick.1.part_ref = bf16[8,256,128]{2,1,0:T(8,128)(2,1)S(1)} custom-call(s32[1]{0:T(128)} %bitcast.place_ref, bf16[8,256,128]{2,1,0:T(8,128)(2,1)S(1)} %copy-done.10, bf16[8,512,128]{2,1,0:T(8,128)(2,1)S(1)} %get-tuple-element.13.key_ref, bf16[8,512,128]{2,1,0:T(8,128)(2,1)S(1)} %copy-done.8, bf16[8,16,128]{2,1,0:T(8,128)(2,1)S(1)} %get-tuple-element.15.bias_ref, ...), custom_call_target="tpu_custom_call" | custom-call | flops 4831838208 | bytes 2621440 | tf_op jit(solution)/shard_map/stick/pallas_call | solution.py:82
  163.8 0.0 copy-start.2
  163.8 0.8 copy-done.2
  164.6 30.7 %gather.1 = bf16[512,2048]{1,0:T(8,128)(2,1)} custom-call(bf16[8,256,128]{2,1,0:T(8,128)(2,1)} %copy-done.2), custom_call_target="tpu_custom_call" | custom-call | bytes 26214400 | tf_op jit(solution)/shard_map/gather/pallas_call | solution.py:449
  195.3 0.0 copy-start.12
  195.3 4.3 %convolution_convert_fusion.2 = bf16[512,512]{1,0:T(8,128)(2,1)} fusion(bf16[512,2048]{1,0:T(8,128)(2,1)} %gather.1, bf16[2048,512]{1,0:T(8,128)(2,1)} %copy-done.6), kind=kOutput, calls=%fused_computation.14 | convolution fusion | flops 1074003968 | bytes 4718592 | tf_op jit(solution)/shard_map/dot_general | solution.py:551
  199.6 0.0 all-to-all-done
  199.6 0.0 copy-done.12
  199.6 1.3 convolution_add_fusion.1
  200.9 1.9 fusion.20
  (3 shorter events, 0.0 us)
Async XLA Ops:
  7.2 66.1 %copy-start = (bf16[1,512,2048]{2,1,0:T(8,128)(2,1)S(1)}, bf16[1,512,2048]{2,1,0:T(8,128)(2,1)}, u32[]{:S(2)}) copy-start(bf16[1,512,2048]{2,1,0:T(8,128)(2,1)} %param.29) | copy-start | bytes 6291460
  7.2 121.5 %reduce-scatter.2.cloned.1.call-start = ((), (), s32[]{:S(2)}) async-start(), calls=%async_computation.2 | async-start | bytes 2621440 | tf_op jit(solution)/shard_map/reduce_scatter | solution.py:554
  14.2 3.3 %copy-start.11 = (bf16[128,2048]{1,0:T(8,128)(2,1)}, bf16[128,2048]{1,0:T(8,128)(2,1)S(1)}, u32[]{:S(2)}) copy-start(bf16[128,2048]{1,0:T(8,128)(2,1)S(1)} %fusion.23) | copy-start | bytes 1572868
  14.2 3.3 %copy-start.1 = (bf16[512,2048]{1,0:T(8,128)(2,1)S(1)}, bf16[512,2048]{1,0:T(8,128)(2,1)}, u32[]{:S(2)}) copy-start(bf16[512,2048]{1,0:T(8,128)(2,1)} %weight_ref.1) | copy-start | bytes 6291460
  14.2 3.3 %copy-start.3 = (bf16[512,512]{1,0:T(8,128)(2,1)S(1)}, bf16[512,512]{1,0:T(8,128)(2,1)}, u32[]{:S(2)}) copy-start(bf16[512,512]{1,0:T(8,128)(2,1)} %query_ref.1) | copy-start | bytes 1572868
  14.2 3.3 %copy-start.4 = (bf16[512,512]{1,0:T(8,128)(2,1)S(1)}, bf16[512,512]{1,0:T(8,128)(2,1)}, u32[]{:S(2)}) copy-start(bf16[512,512]{1,0:T(8,128)(2,1)} %key_ref.1) | copy-start | bytes 1572868
  14.2 3.3 %copy-start.5 = (bf16[512,512]{1,0:T(8,128)(2,1)S(1)}, bf16[512,512]{1,0:T(8,128)(2,1)}, u32[]{:S(2)}) copy-start(bf16[512,512]{1,0:T(8,128)(2,1)} %value_ref.1) | copy-start | bytes 1572868
  17.5 51.9 %copy-start.13 = (bf16[1,2048,512]{2,1,0:T(8,128)(2,1)S(1)}, bf16[1,2048,512]{2,1,0:T(8,128)(2,1)}, u32[]{:S(2)}) copy-start(bf16[1,2048,512]{2,1,0:T(8,128)(2,1)} %param.27) | copy-start | bytes 6291460
  69.3 1.4 copy-start.6
  69.3 1.6 copy-start.7
  69.4 1.8 copy-start.9
  69.4 2.9 %copy-start.14 = (bf16[1,2048,512]{2,1,0:T(8,128)(2,1)S(1)}, bf16[1,2048,512]{2,1,0:T(8,128)(2,1)}, u32[]{:S(2)}) copy-start(bf16[1,2048,512]{2,1,0:T(8,128)(2,1)} %param.28) | copy-start | bytes 6291460
  130.5 69.2 %all-to-all-start = ((bf16[512,8,48]{0,2,1:T(8,128)(2,1)}), bf16[512,8,48]{0,2,1:T(8,128)(2,1)}, u32[]{:S(2)}, u32[]{:S(2)}) async-start(bf16[512,8,48]{0,2,1:T(8,128)(2,1)} %bitcast.64), calls=%async_computation.1 | async-start | bytes 786432 | tf_op jit(solution)/shard_map/all_to_all | solution.py:562
  136.0 1.2 copy-start.8
  137.2 1.0 copy-start.10
  163.8 0.8 copy-start.2
  195.3 4.3 %copy-start.12 = (bf16[384,128]{1,0:T(8,128)(2,1)S(1)}, bf16[384,128]{1,0:T(8,128)(2,1)}, u32[]{:S(2)}) copy-start(bf16[384,128]{1,0:T(8,128)(2,1)} %get-tuple-element.19) | copy-start | bytes 294916
Sparse Core Ops, SparseCore 0:
  82.8 45.8 reduce-scatter.1

commit v3 on v2

--- a/solution.py
+++ b/solution.py
@@ -14,11 +14,57 @@
 MESH = pl.DeviceIdType.MESH
 
 
-def attention_kernel(place_ref, query_ref, key_ref, value_ref, bias_ref, tri_ref, out_ref):
+def attention_kernel(
+    tp_count,
+    query_ref,
+    key_ref,
+    value_ref,
+    bias_ref,
+    tri_ref,
+    partial_ref,
+    out_ref,
+    partial_out,
+    local_sem,
+    send_sem,
+    recv_sem,
+):
     block = pl.program_id(0)
+    own_tp = lax.axis_index("tp")
+    width_out = partial_out.shape[2]
+    local = pltpu.make_async_copy(
+        partial_ref.at[:, columns(own_tp, width_out)], partial_out.at[own_tp], local_sem.at[0]
+    )
+
+    def piece(i, arriving):
+        other = lax.rem(own_tp + i, tp_count)
+        return pltpu.make_async_remote_copy(
+            src_ref=partial_ref.at[:, columns(other, width_out)],
+            dst_ref=partial_out.at[other if arriving else own_tp],
+            send_sem=send_sem.at[other],
+            recv_sem=recv_sem.at[other if arriving else own_tp],
+            device_id={"tp": other},
+            device_id_type=MESH,
+        )
+
+    @pl.when(block == 0)
+    def _():
+        barrier = pltpu.get_barrier_semaphore()
+        for i in range(1, tp_count):
+            pl.semaphore_signal(
+                barrier,
+                inc=1,
+                device_id={"tp": lax.rem(own_tp + i, tp_count)},
+                device_id_type=MESH,
+            )
+        pl.semaphore_wait(barrier, tp_count - 1)
+        for i in range(1, tp_count):
+            piece(i, False).start()
+        local.start()
+
     share, size = query_ref.shape[1:]
     span = key_ref.shape[1]
-    offset = place_ref[0] * share
+    groups = span // share
+    offset = lax.rem(lax.axis_index("ep"), groups) * share
     width = tri_ref.shape[0]
     query = query_ref[block]
     scale = size ** (-0.5) * LOG2E
@@ -70,31 +116,70 @@
     carry = lax.fori_loop(0, block, lambda i, c: unit(block - 1 - i, c, False), carry)
     out_ref[0] = carry[0].astype(out_ref.dtype)
 
-
-def attention(query, key, value, bias, place):
+    @pl.when(block == pl.num_programs(0) - 1)
+    def _():
+        local.wait()
+        for i in range(1, tp_count):
+            piece(i, True).wait_recv()
+        for i in range(1, tp_count):
+            piece(i, False).wait_send()
+
+
+def attention(query, key, value, bias, partial, tp_count):
     blocks, share, size = query.shape
     span = key.shape[1]
     width = min(256, span)
     index = jnp.arange(width)
     tri = (index[:, None] > index[None, :]).astype(jnp.bfloat16)
+    dma = pltpu.SemaphoreType.DMA
     work = blocks * (blocks + 1) // 2 * share * span
     whole = pl.BlockSpec(memory_space=pltpu.VMEM)
     return pl.pallas_call(
-        attention_kernel,
+        functools.partial(attention_kernel, tp_count),
         grid=(blocks,),
-        in_specs=[pl.BlockSpec(memory_space=pltpu.SMEM)] + [whole] * 5,
-        out_specs=pl.BlockSpec((1, share, size), lambda i: (i, 0, 0)),
-        out_shape=jax.ShapeDtypeStruct((blocks, share, size), jnp.bfloat16),
+        in_specs=[whole] * 6,
+        out_specs=[
+            pl.BlockSpec((1, share, size), lambda i: (i, 0, 0)),
+            pl.BlockSpec(memory_space=pl.ANY),
+        ],
+        out_shape=[
+            jax.ShapeDtypeStruct((blocks, share, size), jnp.bfloat16),
+            jax.ShapeDtypeStruct(
+                (tp_count, partial.shape[0], partial.shape[1] // tp_count), jnp.bfloat16
+            ),
+        ],
+        scratch_shapes=[dma((1,)), dma((tp_count,)), dma((tp_count,))],
         cost_estimate=pl.CostEstimate(
             flops=work * (4 * size + 2 * width),
             bytes_accessed=key.size * 5,
             transcendentals=3 * work,
         ),
         compiler_params=pltpu.CompilerParams(
-            dimension_semantics=("arbitrary",), vmem_limit_bytes=40 * 1024 * 1024
+            dimension_semantics=("arbitrary",),
+            vmem_limit_bytes=40 * 1024 * 1024,
+            collective_id=2,
+            has_side_effects=True,
         ),
         name="stick",
-    )(place, query, key, value, bias, tri)
+    )(query, key, value, bias, tri, partial)
+
+
+def others_across(own_tp, tp_count):
+    pair = 2 - tp_count % 2
+    chips = tp_count // pair
+    return [
+        lax.rem(own_tp // pair + i, chips) * pair + lax.rem(own_tp, pair) for i in range(1, chips)
+    ]
+
+
+def beside(own_tp, tp_count):
+    if tp_count % 2:
+        return []
+    return [own_tp + 1 - 2 * lax.rem(own_tp, 2)]
+
+
+def near_first(own_tp, tp_count):
+    return others_across(own_tp, tp_count) + beside(own_tp, tp_count)
 
 
 def columns(index, width):
@@ -138,6 +223,7 @@
     rows_recv,
     relay_send,
     relay_recv,
+    pass_send,
     weight_send,
     weight_recv,
 ):
@@ -254,8 +340,7 @@
             other,
         ).wait_recv()
     local[0].wait()
-    for i in range(1, tp_count):
-        other = lax.rem(own_tp + i, tp_count)
+    for other in near_first(own_tp, tp_count):
         start(remote(rows_own, rows_own, relay_send.at[other], relay_recv.at[own_tp], "tp", other))
     for i in range(1, tp_count):
         other = lax.rem(own_tp + i, tp_count)
@@ -293,6 +378,19 @@
                         own_head * groups + group,
                     )
                 )
+    def rows_arrival(slot):
+        arrived = rows_out.at[:, :, columns(slot, col_count)]
+        remote(
+            arrived, arrived, relay_send.at[slot], relay_recv.at[slot], "tp", slot
+        ).wait_recv()
+        return arrived
+
+    for slot in others_across(own_tp, tp_count):
+        arrived = rows_arrival(slot)
+        for other in beside(own_tp, tp_count):
+            start(
+                remote(arrived, arrived, pass_send.at[slot], relay_recv.at[slot], "tp", other)
+            )
     for i in range(heads):
         for step in range(1, groups):
             group = lax.rem(own_group + step, groups)
@@ -311,14 +409,14 @@
         ).wait_recv()
     for i in range(1, tp_count):
         other = lax.rem(own_tp + i, tp_count)
-        arrived = rows_out.at[:, :, columns(other, col_count)]
-        remote(
-            arrived, arrived, relay_send.at[other], relay_recv.at[other], "tp", other
-        ).wait_recv()
         target = weight_out.at[columns(other, depth), :]
         remote(
             target, target, weight_send.at[other], weight_recv.at[other], "tp", other
         ).wait_recv()
+    for other in beside(own_tp, tp_count):
+        rows_arrival(other)
+        for slot in others_across(other, tp_count):
+            rows_arrival(slot)
     for copy in sent:
         copy.wait_send()
     for copy in local[1:]:
@@ -359,6 +457,7 @@
             dma((tp_count,)),
             dma((tp_count,)),
             dma((tp_count,)),
+            dma((tp_count,)),
         ],
         compiler_params=pltpu.CompilerParams(
             collective_id=0, has_side_effects=True, vmem_limit_bytes=40 * 1024 * 1024
@@ -367,7 +466,21 @@
     )(queries, keys, values, bias, rows, weight)
 
 
-def gather_kernel(counts, part_ref, out_ref, local_sem, send_sem, recv_sem, relay_send, relay_recv):
+def gather_kernel(
+    counts,
+    part_ref,
+    back_ref,
+    out_ref,
+    back_out,
+    local_sem,
+    send_sem,
+    recv_sem,
+    relay_send,
+    relay_recv,
+    pass_send,
+    back_send,
+    back_recv,
+):
     ep_count, tp_count, heads = counts
     groups = ep_count // heads
     share, size = part_ref.shape[1:]
@@ -391,21 +504,40 @@
     meet(ep_count, tp_count)
     local = pltpu.make_async_copy(part_ref.at[own], place_of(own, own_tp), local_sem.at[0])
     local.start()
+    local_back = pltpu.make_async_copy(back_ref.at[own], back_out.at[own], local_sem.at[1])
+    local_back.start()
     sent = []
+
+    def start(copy):
+        copy.start()
+        sent.append(copy)
+
     for i in range(1, ep_count):
         other = lax.rem(own + i, ep_count)
-        copy = remote(
-            part_ref.at[other],
-            place_of(own, own_tp),
-            send_sem.at[other],
-            recv_sem.at[own],
-            "ep",
-            other,
-        )
-        copy.start()
-        sent.append(copy)
-    for i in range(ep_count):
-        source = lax.rem(own + ep_count - i, ep_count)
+        start(
+            remote(
+                part_ref.at[other],
+                place_of(own, own_tp),
+                send_sem.at[other],
+                recv_sem.at[own],
+                "ep",
+                other,
+            )
+        )
+    for i in range(1, ep_count):
+        other = lax.rem(own + i, ep_count)
+        start(
+            remote(
+                back_ref.at[other],
+                back_out.at[own],
+                back_send.at[other],
+                back_recv.at[own],
+                "ep",
+                other,
+            )
+        )
+    sources = [lax.rem(own + ep_count - i, ep_count) for i in range(ep_count)]
+    for i, source in enumerate(sources):
         piece = place_of(source, own_tp)
         if i == 0:
             local.wait()
@@ -413,59 +545,88 @@
             remote(
                 piece, piece, send_sem.at[source], recv_sem.at[source], "ep", source
             ).wait_recv()
-        for j in range(1, tp_count):
-            other = lax.rem(own_tp + j, tp_count)
-            copy = remote(
-                piece,
-                piece,
-                relay_send.at[source, other],
-                relay_recv.at[source, own_tp],
-                "tp",
-                other,
-            )
-            copy.start()
-            sent.append(copy)
-    for i in range(ep_count):
-        source = lax.rem(own + ep_count - i, ep_count)
-        for j in range(1, tp_count):
-            other = lax.rem(own_tp + j, tp_count)
-            piece = place_of(source, other)
-            remote(
-                piece,
-                piece,
-                relay_send.at[source, other],
-                relay_recv.at[source, other],
-                "tp",
-                other,
-            ).wait_recv()
+        for other in near_first(own_tp, tp_count):
+            start(
+                remote(
+                    piece,
+                    piece,
+                    relay_send.at[source, other],
+                    relay_recv.at[source, own_tp],
+                    "tp",
+                    other,
+                )
+            )
+
+    def arrival(source, slot):
+        piece = place_of(source, slot)
+        remote(
+            piece, piece, relay_send.at[source, slot], relay_recv.at[source, slot], "tp", slot
+        ).wait_recv()
+        return piece
+
+    for source in sources:
+        for slot in others_across(own_tp, tp_count):
+            piece = arrival(source, slot)
+            for other in beside(own_tp, tp_count):
+                start(
+                    remote(
+                        piece,
+                        piece,
+                        pass_send.at[source, slot],
+                        relay_recv.at[source, slot],
+                        "tp",
+                        other,
+                    )
+                )
+    for source in sources:
+        for other in beside(own_tp, tp_count):
+            arrival(source, other)
+            for slot in others_across(other, tp_count):
+                arrival(source, slot)
+    for source in sources[1:]:
+        remote(
+            back_ref.at[source],
+            back_out.at[source],
+            back_send.at[source],
+            back_recv.at[source],
+            "ep",
+            source,
+        ).wait_recv()
     for copy in sent:
         copy.wait_send()
-
-
-def gather(parts, counts):
+    local_back.wait()
+
+
+def gather(parts, back, counts):
     ep_count, tp_count, heads = counts
     _, share, size = parts.shape
     dma = pltpu.SemaphoreType.DMA
     return pl.pallas_call(
         functools.partial(gather_kernel, counts),
-        in_specs=[pl.BlockSpec(memory_space=pltpu.VMEM)],
-        out_specs=pl.BlockSpec(memory_space=pl.ANY),
-        out_shape=jax.ShapeDtypeStruct(
-            (share * ep_count // heads, tp_count * heads * size), jnp.bfloat16
-        ),
+        in_specs=[pl.BlockSpec(memory_space=pltpu.VMEM)] * 2,
+        out_specs=[pl.BlockSpec(memory_space=pl.ANY)] * 2,
+        out_shape=[
+            jax.ShapeDtypeStruct(
+                (share * ep_count // heads, tp_count * heads * size), jnp.bfloat16
+            ),
+            jax.ShapeDtypeStruct(back.shape, jnp.bfloat16),
+        ],
         scratch_shapes=[
-            dma((1,)),
+            dma((2,)),
             dma((ep_count,)),
             dma((ep_count,)),
             dma((ep_count, tp_count)),
             dma((ep_count, tp_count)),
+            dma((ep_count, tp_count)),
+            dma((ep_count,)),
+            dma((ep_count,)),
         ],
         compiler_params=pltpu.CompilerParams(collective_id=1, has_side_effects=True),
         cost_estimate=pl.CostEstimate(
             flops=0, bytes_accessed=parts.size * 100, transcendentals=0
         ),
         name="gather",
-    )(parts)
+    )(parts, back)
 
 
 def body(
@@ -490,9 +651,6 @@
     size = queries.shape[1] // heads
     ep_count = lax.axis_size("ep")
     tp_count = lax.axis_size("tp")
-    groups = ep_count // heads
-    share = span // groups
-    place = (lax.axis_index("ep") % groups).astype(jnp.int32).reshape(1)
 
     counts = (ep_count, tp_count, heads)
     col_count = out_weight.shape[1] // tp_count
@@ -541,34 +699,32 @@
     up_sum = jnp.einsum("secd,edf->secf", grid, expert_up, preferred_element_type=jnp.float32)
     expert_hidden = (jax.nn.silu(gate_sum) * up_sum).astype(jnp.bfloat16)
     routed = jnp.einsum(
-        "secf,efd->dsec", expert_hidden, expert_down, preferred_element_type=jnp.float32
-    ).reshape(tp_count * col_count, -1)
-    common = jnp.einsum("tf,fd->dt", shared_hidden, shared_down, preferred_element_type=jnp.float32)
-    partial = jnp.concatenate([routed, common], axis=1).astype(jnp.bfloat16)
-    partial, query_all = lax.optimization_barrier((partial, query_all))
-    mixed_heads = attention(query_all, key_all, value_all, bias_all, place)
-    heads_all = gather(mixed_heads, counts)
+        "secf,efd->secd", expert_hidden, expert_down, preferred_element_type=jnp.float32
+    ).reshape(send_slots, -1)
+    common = jnp.dot(shared_hidden, shared_down, preferred_element_type=jnp.float32)
+    partial = jnp.concatenate([routed, common], axis=0).astype(jnp.bfloat16)
+    mixed_heads, partial_all = attention(
+        query_all, key_all, value_all, bias_all, partial, tp_count
+    )
+    expert_sum = jnp.sum(partial_all.astype(jnp.float32), axis=0)
+    routed_sum = expert_sum[:send_slots].astype(jnp.bfloat16)
+    common_sum = expert_sum[send_slots:]
+    heads_all, returned = gather(
+        mixed_heads, routed_sum.reshape(ep_count, local_experts * capacity, col_count), counts
+    )
+    returned = returned.reshape(send_slots, col_count)
     mixed_tokens = jnp.dot(heads_all, weight_cols, preferred_element_type=jnp.float32).astype(
         jnp.bfloat16
     )
-    expert_sum = lax.psum_scatter(
-        partial,
-        "tp",
-        scatter_dimension=0,
-        tiled=True,
-    )
-    routed_sum = expert_sum[:, :send_slots]
-    common_sum = expert_sum[:, send_slots:].astype(jnp.float32)
-    returned = lax.all_to_all(routed_sum, "ep", split_axis=1, concat_axis=1, tiled=True)
     gates = route_scores / jnp.sum(route_scores, axis=-1, keepdims=True) * ROUTED_SCALE
     gates_high = gates.astype(jnp.bfloat16)
     gates_low = (gates - gates_high.astype(jnp.float32)).astype(jnp.bfloat16)
 
     def combined(part):
         table = jnp.sum(jnp.where(matches, part[None], jnp.bfloat16(0)), axis=2)
-        return jnp.einsum("ds,st->td", returned, table, preferred_element_type=jnp.float32)
-
-    expert_mix = (common_sum.T + combined(gates_high) + combined(gates_low)).astype(jnp.bfloat16)
+        return jnp.einsum("st,sd->td", table, returned, preferred_element_type=jnp.float32)
+
+    expert_mix = (common_sum + combined(gates_high) + combined(gates_low)).astype(jnp.bfloat16)
     return (mixed_tokens, expert_mix)
 
 

time: 210 us -> 156 us (0.74)
  the two profiles are of different devices: /device:TPU:0 before, /device:TPU:31 now
where the time goes in v3:
time: 156 us
  Pallas kernels  114 us (73%)
  matrix products  20.9 us (13%)
  local copies, waits for them, and re-layouts  11.1 us (7%)
  other arithmetic  8.93 us (6%)
    pallas_call x1, Pallas kernels, exchange(): pl.pallas_call(functools.partial(exchange_kernel, counts), in_specs=[whol...  52.8 us
    pallas_call x1, Pallas kernels, gather(): pl.pallas_call(functools.partial(gather_kernel, counts), in_specs=[pl.Blo...  33.3 us
    pallas_call x1, Pallas kernels, attention(): pl.pallas_call(functools.partial(attention_kernel, tp_count), grid=(block...  27.9 us
    unnamed x38, local copies, waits for them, and re-layouts  9.58 us
    dot_general x1, matrix products, body(): jnp.einsum('secf,efd->secd', expert_hidden, expert_down, preferred_elemen...  5.35 us
    dot_general x1, matrix products, body(): jnp.dot(heads_all, weight_cols, preferred_element_type=jnp.float32)  4.32 us
    dot_general x1, matrix products, body(): jnp.dot(shared_hidden, shared_down, preferred_element_type=jnp.float32)  4.25 us

profile of v3, /device:TPU:31, one launch (start us, length us, event | category | flops | bytes accessed | tf_op | source)
XLA Modules:
  0.0 155.7 jit_solution(10733685080055319524)
XLA Ops:
  0.6 0.0 copy-start
  0.6 1.4 fusion.22
  2.0 0.7 reduce_sum.89
  2.7 0.7 subtract_convert_fusion
  3.4 0.7 fusion.48
  4.1 0.1 convolution_convert_fusion.4
  4.2 0.7 select_reduce_fusion
  5.0 0.7 multiply_add_fusion
  5.6 0.7 reshape.56
  6.4 0.7 fusion.44
  7.1 1.2 fusion.24
  8.3 0.0 copy-start.14
  8.4 0.8 copy-done.14
  9.1 2.7 %fusion.52 = f32[128,512]{1,0:T(8,128)} fusion(bf16[128,2048]{1,0:T(8,128)(2,1)S(1)} %fusion.24, bf16[2048,512]{1,0:T(8,128)(2,1)} %param.24), kind=kOutput, calls=%fused_computation.62 | convolution fusion | flops 268435456 | bytes 2883584 | tf_op jit(solution)/shard_map/dot_general | solution.py:667
  11.9 0.0 copy-start.3
  11.9 0.0 copy-start.4
  11.9 4.2 %convolution_convert_fusion.1 = bf16[128,2048]{1,0:T(8,128)(2,1)} fusion(bf16[512,2048]{1,0:T(8,128)(2,1)} %param.26, bf16[128,2048]{1,0:T(8,128)(2,1)} %copy-done.14, bf16[2048,512]{1,0:T(8,128)(2,1)} %param.25, f32[128,512]{1,0:T(8,128)} %fusion.52), kind=kOutput, calls=%fused_computation.2 | convolution fusion | flops 537526272 | bytes 5505024 | tf_op jit(solution)/shard_map/dot_general | solution.py:704
  16.1 1.1 convolution_convert_fusion.3
  17.3 0.0 copy-done.3
  17.3 0.0 copy-done.4
  17.3 0.0 copy-start.1
  17.3 1.6 %copy-done.1 = bf16[512,2048]{1,0:T(8,128)(2,1)S(1)} copy-done((bf16[512,2048]{1,0:T(8,128)(2,1)S(1)}, bf16[512,2048]{1,0:T(8,128)(2,1)}, u32[]{:S(2)}) %copy-start.1) | copy-done | bytes 2097176
  18.9 0.0 copy-start.5
  18.9 1.0 copy-done.5
  19.9 0.0 copy-start.18
  19.9 52.8 %exchange.1 = (bf16[8,256,128]{2,1,0:T(8,128)(2,1)S(1)}, bf16[8,512,128]{2,1,0:T(8,128)(2,1)S(1)}, bf16[8,512,128]{2,1,0:T(8,128)(2,1)S(1)}, bf16[8,16,128]{2,1,...) custom-call(bf16[512,512]{1,0:T(8,128)(2,1)S(1)} %copy-done.3, ...), custom_call_target="tpu_custom_call" | custom-call | tf_op jit(solution)/shard_map/exchange/pallas_call | solution.py:436
  72.8 0.0 copy-start.6
  72.8 1.3 copy-done.6
  74.1 0.0 copy-start.8
  74.1 1.0 copy-done.8
  75.1 0.0 copy-start.10
  75.1 1.0 copy-done.10
  76.1 0.0 copy-start.12
  76.1 0.8 copy-done.12
  76.9 0.0 copy-start.7
  76.9 1.2 copy-done.7
  78.1 0.0 copy-done.18
  78.1 1.9 %fusion.5 = f32[8,1,48,512]{3,2,0,1:T(8,128)} fusion(bf16[8,48,2048]{2,1,0:T(8,128)(2,1)S(1)} %get-tuple-element.16, bf16[1,2048,512]{2,1,0:T(8,128)(2,1)S(1)} %copy-done.18), kind=kOutput, calls=%fused_computation.11 | convolution fusion | flops 805306368 | bytes 4456448 | tf_op jit(solution)/shard_map/secd,edf->secf/dot_general | solution.py:698
  79.9 0.0 copy-done
  79.9 0.0 copy-start.15
  80.0 5.3 %convolution_convert_fusion = bf16[8,48,2048]{2,1,0:T(8,128)(2,1)} fusion(bf16[1,512,2048]{2,1,0:T(8,128)(2,1)S(1)} %copy-done, bf16[8,48,2048]{2,1,0:T(8,128)(2,1)} %copy-done.7, bf16[1,2048,512]{2,1,0:T(8,128)(2,1)} %param.28, f32[8,1,48,512]{3,2,0,1:T(8,128)} %fusion.5), kind=kOutput, calls=%fused_computation.1 | convolution fusion | flops 1612578816 | bytes 8126464 | tf_op jit(solution)/shard_map/secf,efd->secd/dot_general | solution.py:701
  85.3 0.0 copy-done.15
  85.3 0.0 copy-start.9
  85.3 0.0 copy-start.11
  85.3 0.0 copy-start.13
  85.3 1.8 %pad_maximum_fusion.partial_ref = bf16[512,2048]{1,0:T(8,128)(2,1)S(1)} fusion(bf16[128,2048]{1,0:T(8,128)(2,1)S(1)} %copy-done.15, bf16[384,2048]{1,0:T(8,128)(2,1)} %bitcast.78), kind=kLoop, calls=%fused_computation.3 | loop fusion | flops 4194304 | bytes 4194304 | tf_op jit(solution)/shard_map/concatenate | solution.py:705
  87.1 0.0 copy-done.9
  87.1 0.2 copy-done.11
  87.3 0.1 copy-done.13
  87.4 27.9 %stick.1 = (bf16[8,256,128]{2,1,0:T(8,128)(2,1)S(1)}, bf16[4,512,512]{2,1,0:T(8,128)(2,1)S(1)}) custom-call(bf16[8,256,128]{2,1,0:T(8,128)(2,1)S(1)} %copy-done.13, bf16[8,512,128]{2,1,0:T(8,128)(2,1)S(1)} %copy-done.9, bf16[8,512,128]{2,1,0:T(8,128)(2,1)S(1)} %copy-done.11, bf16[8,16,128]{2,1,0:T(8,128)(2,1)S(1)} %get-tuple-element.15.bias_ref, ...), custom_call_target="tpu_custom_call" | custom-call | flops 4831838208 | bytes 2621440 | tf_op jit(solution)/shard_map/stick/pallas_call | solution.py:137
  115.3 0.0 copy-start.2
  115.4 0.3 convert_reduce_fusion
  115.7 0.5 copy-done.2
  116.1 0.8 slice.13
  116.9 33.3 %gather.1 = (bf16[512,2048]{1,0:T(8,128)(2,1)}, bf16[8,48,512]{2,1,0:T(8,128)(2,1)}) custom-call(bf16[8,256,128]{2,1,0:T(8,128)(2,1)} %copy-done.2, bf16[8,48,512]{2,1,0:T(8,128)(2,1)} %bitcast.77), custom_call_target="tpu_custom_call" | custom-call | bytes 26214400 | tf_op jit(solution)/shard_map/gather/pallas_call | solution.py:604
  150.2 0.0 copy-start.16
  150.2 0.0 copy-start.17
  150.2 4.3 %convolution_convert_fusion.2 = bf16[512,512]{1,0:T(8,128)(2,1)} fusion(bf16[512,2048]{1,0:T(8,128)(2,1)} %get-tuple-element.19, bf16[2048,512]{1,0:T(8,128)(2,1)} %copy-done.6), kind=kOutput, calls=%fused_computation.13 | convolution fusion | flops 1074003968 | bytes 4718592 | tf_op jit(solution)/shard_map/dot_general | solution.py:716
  154.5 0.0 copy-done.16
  154.5 0.0 copy-done.17
  154.5 0.3 convolution_add_fusion.1
  154.8 0.9 fusion.21
  (3 shorter events, 0.0 us)
Async XLA Ops:
  0.6 79.3 %copy-start = (bf16[1,512,2048]{2,1,0:T(8,128)(2,1)S(1)}, bf16[1,512,2048]{2,1,0:T(8,128)(2,1)}, u32[]{:S(2)}) copy-start(bf16[1,512,2048]{2,1,0:T(8,128)(2,1)} %param.29) | copy-start | bytes 6291460
  8.3 0.8 copy-start.14
  11.9 5.4 %copy-start.3 = (bf16[512,512]{1,0:T(8,128)(2,1)S(1)}, bf16[512,512]{1,0:T(8,128)(2,1)}, u32[]{:S(2)}) copy-start(bf16[512,512]{1,0:T(8,128)(2,1)} %query_ref.1) | copy-start | bytes 1572868
  11.9 5.4 %copy-start.4 = (bf16[512,512]{1,0:T(8,128)(2,1)S(1)}, bf16[512,512]{1,0:T(8,128)(2,1)}, u32[]{:S(2)}) copy-start(bf16[512,512]{1,0:T(8,128)(2,1)} %key_ref.1) | copy-start | bytes 1572868
  17.3 1.6 %copy-start.1 = (bf16[512,2048]{1,0:T(8,128)(2,1)S(1)}, bf16[512,2048]{1,0:T(8,128)(2,1)}, u32[]{:S(2)}) copy-start(bf16[512,2048]{1,0:T(8,128)(2,1)} %weight_ref.1) | copy-start | bytes 6291460
  18.9 1.0 copy-start.5
  19.9 58.2 %copy-start.18 = (bf16[1,2048,512]{2,1,0:T(8,128)(2,1)S(1)}, bf16[1,2048,512]{2,1,0:T(8,128)(2,1)}, u32[]{:S(2)}) copy-start(bf16[1,2048,512]{2,1,0:T(8,128)(2,1)} %param.27) | copy-start | bytes 6291460
  72.8 1.3 copy-start.6
  74.1 1.0 copy-start.8
  75.1 1.0 copy-start.10
  76.1 0.8 copy-start.12
  76.9 1.2 copy-start.7
  79.9 5.4 %copy-start.15 = (bf16[128,2048]{1,0:T(8,128)(2,1)S(1)}, bf16[128,2048]{1,0:T(8,128)(2,1)}, u32[]{:S(2)}) copy-start(bf16[128,2048]{1,0:T(8,128)(2,1)} %convolution_convert_fusion.1) | copy-start | bytes 1572868
  85.3 1.8 %copy-start.9 = (bf16[8,512,128]{2,1,0:T(8,128)(2,1)S(1)}, bf16[8,512,128]{2,1,0:T(8,128)(2,1)}, u32[]{:S(2)}) copy-start(bf16[8,512,128]{2,1,0:T(8,128)(2,1)} %copy-done.8) | copy-start | bytes 3145732
  85.3 2.0 %copy-start.11 = (bf16[8,512,128]{2,1,0:T(8,128)(2,1)S(1)}, bf16[8,512,128]{2,1,0:T(8,128)(2,1)}, u32[]{:S(2)}) copy-start(bf16[8,512,128]{2,1,0:T(8,128)(2,1)} %copy-done.10) | copy-start | bytes 3145732
  85.3 2.1 %copy-start.13 = (bf16[8,256,128]{2,1,0:T(8,128)(2,1)S(1)}, bf16[8,256,128]{2,1,0:T(8,128)(2,1)}, u32[]{:S(2)}) copy-start(bf16[8,256,128]{2,1,0:T(8,128)(2,1)} %copy-done.12) | copy-start | bytes 1572868
  115.3 0.8 copy-start.2
  150.2 4.3 %copy-start.16 = (bf16[8,48,512]{2,1,0:T(8,128)(2,1)S(1)}, bf16[8,48,512]{2,1,0:T(8,128)(2,1)}, u32[]{:S(2)}) copy-start(bf16[8,48,512]{2,1,0:T(8,128)(2,1)} %get-tuple-element.21) | copy-start | bytes 1179652
  150.2 4.3 %copy-start.17 = (bf16[384,128]{1,0:T(8,128)(2,1)S(1)}, bf16[384,128]{1,0:T(8,128)(2,1)}, u32[]{:S(2)}) copy-start(bf16[384,128]{1,0:T(8,128)(2,1)} %get-tuple-element.23) | copy-start | bytes 294916

commit v4 on v3

--- a/solution.py
+++ b/solution.py
@@ -24,11 +24,16 @@
     partial_ref,
     out_ref,
     partial_out,
+    out_buf,
     local_sem,
     send_sem,
     recv_sem,
+    out_send,
+    out_recv,
 ):
     block = pl.program_id(0)
+    ep_count = key_ref.shape[0]
+    own = lax.axis_index("ep")
     own_tp = lax.axis_index("tp")
     width_out = partial_out.shape[2]
     local = pltpu.make_async_copy(
@@ -48,15 +53,7 @@
 
     @pl.when(block == 0)
     def _():
-        barrier = pltpu.get_barrier_semaphore()
-        for i in range(1, tp_count):
-            pl.semaphore_signal(
-                barrier,
-                inc=1,
-                device_id={"tp": lax.rem(own_tp + i, tp_count)},
-                device_id_type=MESH,
-            )
-        pl.semaphore_wait(barrier, tp_count - 1)
+        meet(ep_count, tp_count)
         for i in range(1, tp_count):
             piece(i, False).start()
         local.start()
@@ -114,11 +111,46 @@
     carry = (jnp.zeros((share, size), jnp.float32), jnp.zeros((share, 1), jnp.float32))
     carry = unit(block, carry, True)
     carry = lax.fori_loop(0, block, lambda i, c: unit(block - 1 - i, c, False), carry)
-    out_ref[0] = carry[0].astype(out_ref.dtype)
+    out_buf[block] = carry[0].astype(out_buf.dtype)
+
+    def place_of(source):
+        return out_ref.at[columns(lax.rem(source, groups), share), columns(source // groups, size)]
+
+    def result(owner, source):
+        return pltpu.make_async_remote_copy(
+            src_ref=out_buf.at[owner],
+            dst_ref=place_of(source),
+            send_sem=out_send.at[owner],
+            recv_sem=out_recv.at[source],
+            device_id={"ep": owner},
+            device_id_type=MESH,
+        )
+
+    local_out = pltpu.make_async_copy(out_buf.at[own], place_of(own), local_sem.at[1])
+
+    def leave(owner):
+        @pl.when(owner == own)
+        def _():
+            local_out.start()
+
+        @pl.when(owner != own)
+        def _():
+            result(owner, own).start()
+
+    @pl.when(block > 0)
+    def _():
+        leave(block - 1)
 
     @pl.when(block == pl.num_programs(0) - 1)
     def _():
         local.wait()
+        leave(block)
+        for i in range(1, ep_count):
+            other = lax.rem(own + i, ep_count)
+            result(other, other).wait_recv()
+        for i in range(1, ep_count):
+            result(lax.rem(own + i, ep_count), own).wait_send()
+        local_out.wait()
         for i in range(1, tp_count):
             piece(i, True).wait_recv()
         for i in range(1, tp_count):
@@ -139,16 +171,23 @@
         grid=(blocks,),
         in_specs=[whole] * 6,
         out_specs=[
-            pl.BlockSpec((1, share, size), lambda i: (i, 0, 0)),
+            pl.BlockSpec(memory_space=pl.ANY),
             pl.BlockSpec(memory_space=pl.ANY),
         ],
         out_shape=[
-            jax.ShapeDtypeStruct((blocks, share, size), jnp.bfloat16),
+            jax.ShapeDtypeStruct((span, blocks * share // span * size), jnp.bfloat16),
             jax.ShapeDtypeStruct(
                 (tp_count, partial.shape[0], partial.shape[1] // tp_count), jnp.bfloat16
             ),
         ],
-        scratch_shapes=[dma((1,)), dma((tp_count,)), dma((tp_count,))],
+        scratch_shapes=[
+            pltpu.VMEM((blocks, share, size), jnp.bfloat16),
+            dma((2,)),
+            dma((tp_count,)),
+            dma((tp_count,)),
+            dma((blocks,)),
+            dma((blocks,)),
+        ],
         cost_estimate=pl.CostEstimate(
             flops=work * (4 * size + 2 * width),
             bytes_accessed=key.size * 5,
@@ -473,8 +512,6 @@
     out_ref,
     back_out,
     local_sem,
-    send_sem,
-    recv_sem,
     relay_send,
     relay_recv,
     pass_send,
@@ -483,13 +520,11 @@
 ):
     ep_count, tp_count, heads = counts
     groups = ep_count // heads
-    share, size = part_ref.shape[1:]
+    depth = part_ref.shape[1]
     own, own_tp = lax.axis_index("ep"), lax.axis_index("tp")
 
-    def place_of(source, slot):
-        return out_ref.at[
-            columns(lax.rem(source, groups), share), columns(slot * heads + source // groups, size)
-        ]
+    def place_of(slot):
+        return out_ref.at[:, columns(slot, depth)]
 
     def remote(source, target, send, recv, axis, device):
         return pltpu.make_async_remote_copy(
@@ -502,7 +537,7 @@
         )
 
     meet(ep_count, tp_count)
-    local = pltpu.make_async_copy(part_ref.at[own], place_of(own, own_tp), local_sem.at[0])
+    local = pltpu.make_async_copy(part_ref, place_of(own_tp), local_sem.at[0])
     local.start()
     local_back = pltpu.make_async_copy(back_ref.at[own], back_out.at[own], local_sem.at[1])
     local_back.start()
@@ -512,15 +547,14 @@
         copy.start()
         sent.append(copy)
 
-    for i in range(1, ep_count):
-        other = lax.rem(own + i, ep_count)
+    for other in near_first(own_tp, tp_count):
         start(
             remote(
-                part_ref.at[other],
-                place_of(own, own_tp),
-                send_sem.at[other],
-                recv_sem.at[own],
-                "ep",
+                part_ref,
+                place_of(own_tp),
+                relay_send.at[other],
+                relay_recv.at[own_tp],
+                "tp",
                 other,
             )
         )
@@ -536,54 +570,23 @@
                 other,
             )
         )
-    sources = [lax.rem(own + ep_count - i, ep_count) for i in range(ep_count)]
-    for i, source in enumerate(sources):
-        piece = place_of(source, own_tp)
-        if i == 0:
-            local.wait()
-        else:
-            remote(
-                piece, piece, send_sem.at[source], recv_sem.at[source], "ep", source
-            ).wait_recv()
-        for other in near_first(own_tp, tp_count):
-            start(
-                remote(
-                    piece,
-                    piece,
-                    relay_send.at[source, other],
-                    relay_recv.at[source, own_tp],
-                    "tp",
-                    other,
-                )
-            )
-
-    def arrival(source, slot):
-        piece = place_of(source, slot)
+    def arrival(slot):
+        piece = place_of(slot)
         remote(
-            piece, piece, relay_send.at[source, slot], relay_recv.at[source, slot], "tp", slot
+            piece, piece, relay_send.at[slot], relay_recv.at[slot], "tp", slot
         ).wait_recv()
         return piece
 
-    for source in sources:
-        for slot in others_across(own_tp, tp_count):
-            piece = arrival(source, slot)
-            for other in beside(own_tp, tp_count):
-                start(
-                    remote(
-                        piece,
-                        piece,
-                        pass_send.at[source, slot],
-                        relay_recv.at[source, slot],
-                        "tp",
-                        other,
-                    )
-                )
-    for source in sources:
+    for slot in others_across(own_tp, tp_count):
+        piece = arrival(slot)
         for other in beside(own_tp, tp_count):
-            arrival(source, other)
-            for slot in others_across(other, tp_count):
-                arrival(source, slot)
-    for source in sources[1:]:
+            start(remote(piece, piece, pass_send.at[slot], relay_recv.at[slot], "tp", other))
+    for other in beside(own_tp, tp_count):
+        arrival(other)
+        for slot in others_across(other, tp_count):
+            arrival(slot)
+    for i in range(1, ep_count):
+        source = lax.rem(own + i, ep_count)
         remote(
             back_ref.at[source],
             back_out.at[source],
@@ -594,12 +597,12 @@
         ).wait_recv()
     for copy in sent:
         copy.wait_send()
+    local.wait()
     local_back.wait()
 
 
 def gather(parts, back, counts):
     ep_count, tp_count, heads = counts
-    _, share, size = parts.shape
     dma = pltpu.SemaphoreType.DMA
     return pl.pallas_call(
         functools.partial(gather_kernel, counts),
@@ -607,17 +610,15 @@
         out_specs=[pl.BlockSpec(memory_space=pl.ANY)] * 2,
         out_shape=[
             jax.ShapeDtypeStruct(
-                (share * ep_count // heads, tp_count * heads * size), jnp.bfloat16
+                (parts.shape[0], tp_count * parts.shape[1]), jnp.bfloat16
             ),
             jax.ShapeDtypeStruct(back.shape, jnp.bfloat16),
         ],
         scratch_shapes=[
             dma((2,)),
-            dma((ep_count,)),
-            dma((ep_count,)),
-            dma((ep_count, tp_count)),
-            dma((ep_count, tp_count)),
-            dma((ep_count, tp_count)),
+            dma((tp_count,)),
+            dma((tp_count,)),
+            dma((tp_count,)),
             dma((ep_count,)),
             dma((ep_count,)),
         ],

time: 156 us -> 159 us (1.019)
  the two profiles are of different devices: /device:TPU:31 before, /device:TPU:0 now
where the time goes in v4:
time: 159 us; the launch traced here: 158 us
  Pallas kernels  117 us (74%)
  matrix products  21 us (13%)
  local copies, waits for them, and re-layouts  11.1 us (7%)
  other arithmetic  8.93 us (6%)
    pallas_call x1, Pallas kernels, exchange(): pl.pallas_call(functools.partial(exchange_kernel, counts), in_specs=[whol...  50.5 us
    pallas_call x1, Pallas kernels, attention(): pl.pallas_call(functools.partial(attention_kernel, tp_count), grid=(block...  38.2 us
    pallas_call x1, Pallas kernels, gather(): pl.pallas_call(functools.partial(gather_kernel, counts), in_specs=[pl.Blo...  27.8 us
    unnamed x38, local copies, waits for them, and re-layouts  9.58 us
    dot_general x1, matrix products, body(): jnp.einsum('secf,efd->secd', expert_hidden, expert_down, preferred_elemen...  5.35 us
    dot_general x1, matrix products, body(): jnp.dot(heads_all, weight_cols, preferred_element_type=jnp.float32)  4.32 us
    dot_general x1, matrix products, body(): jnp.dot(shared_hidden, shared_down, preferred_element_type=jnp.float32)  4.25 us

profile of v4, /device:TPU:0, one launch (start us, length us, event | category | flops | bytes accessed | tf_op | source)
XLA Modules:
  0.0 158.3 jit_solution(14727110163323168710)
XLA Ops:
  0.6 0.0 copy-start
  0.6 1.4 fusion.22
  2.0 0.7 reduce_sum.89
  2.7 0.7 subtract_convert_fusion
  3.4 0.7 fusion.48
  4.1 0.1 convolution_convert_fusion.4
  4.2 0.7 select_reduce_fusion
  5.0 0.7 multiply_add_fusion
  5.6 0.7 reshape.56
  6.4 0.7 fusion.44
  7.1 1.2 fusion.24
  8.3 0.0 copy-start.14
  8.4 0.8 copy-done.14
  9.1 2.7 %fusion.52 = f32[128,512]{1,0:T(8,128)} fusion(bf16[128,2048]{1,0:T(8,128)(2,1)S(1)} %fusion.24, bf16[2048,512]{1,0:T(8,128)(2,1)} %param.24), kind=kOutput, calls=%fused_computation.62 | convolution fusion | flops 268435456 | bytes 2883584 | tf_op jit(solution)/shard_map/dot_general | solution.py:668
  11.9 0.0 copy-start.3
  11.9 0.0 copy-start.4
  11.9 4.3 %convolution_convert_fusion.1 = bf16[128,2048]{1,0:T(8,128)(2,1)} fusion(bf16[512,2048]{1,0:T(8,128)(2,1)} %param.26, bf16[128,2048]{1,0:T(8,128)(2,1)} %copy-done.14, bf16[2048,512]{1,0:T(8,128)(2,1)} %param.25, f32[128,512]{1,0:T(8,128)} %fusion.52), kind=kOutput, calls=%fused_computation.2 | convolution fusion | flops 537526272 | bytes 5505024 | tf_op jit(solution)/shard_map/dot_general | solution.py:705
  16.1 1.1 convolution_convert_fusion.3
  17.3 0.0 copy-done.3
  17.3 0.0 copy-done.4
  17.3 0.0 copy-start.1
  17.3 1.6 copy-done.1
  18.9 0.0 copy-start.5
  18.9 1.0 copy-done.5
  19.9 0.0 copy-start.18
  19.9 50.5 %exchange.1 = (bf16[8,256,128]{2,1,0:T(8,128)(2,1)S(1)}, bf16[8,512,128]{2,1,0:T(8,128)(2,1)S(1)}, bf16[8,512,128]{2,1,0:T(8,128)(2,1)S(1)}, bf16[8,16,128]{2,1,...) custom-call(bf16[512,512]{1,0:T(8,128)(2,1)S(1)} %copy-done.3, ...), custom_call_target="tpu_custom_call" | custom-call | tf_op jit(solution)/shard_map/exchange/pallas_call | solution.py:475
  70.5 0.0 copy-start.6
  70.5 1.3 copy-done.6
  71.8 0.0 copy-start.8
  71.8 1.0 copy-done.8
  72.8 0.0 copy-start.10
  72.8 1.0 copy-done.10
  73.8 0.0 copy-start.12
  73.8 0.8 copy-done.12
  74.6 0.0 copy-start.7
  74.6 1.2 copy-done.7
  75.8 0.0 copy-done.18
  75.8 1.9 %fusion.5 = f32[8,1,48,512]{3,2,0,1:T(8,128)} fusion(bf16[8,48,2048]{2,1,0:T(8,128)(2,1)S(1)} %get-tuple-element.16, bf16[1,2048,512]{2,1,0:T(8,128)(2,1)S(1)} %copy-done.18), kind=kOutput, calls=%fused_computation.11 | convolution fusion | flops 805306368 | bytes 4456448 | tf_op jit(solution)/shard_map/secd,edf->secf/dot_general | solution.py:699
  77.7 0.0 copy-done
  77.7 0.0 copy-start.15
  77.7 5.3 %convolution_convert_fusion = bf16[8,48,2048]{2,1,0:T(8,128)(2,1)} fusion(bf16[1,512,2048]{2,1,0:T(8,128)(2,1)S(1)} %copy-done, bf16[8,48,2048]{2,1,0:T(8,128)(2,1)} %copy-done.7, bf16[1,2048,512]{2,1,0:T(8,128)(2,1)} %param.28, f32[8,1,48,512]{3,2,0,1:T(8,128)} %fusion.5), kind=kOutput, calls=%fused_computation.1 | convolution fusion | flops 1612578816 | bytes 8126464 | tf_op jit(solution)/shard_map/secf,efd->secd/dot_general | solution.py:702
  83.0 0.0 copy-done.15
  83.0 0.0 copy-start.9
  83.0 0.0 copy-start.11
  83.0 0.0 copy-start.13
  83.0 1.8 %pad_maximum_fusion.partial_ref = bf16[512,2048]{1,0:T(8,128)(2,1)S(1)} fusion(bf16[128,2048]{1,0:T(8,128)(2,1)S(1)} %copy-done.15, bf16[384,2048]{1,0:T(8,128)(2,1)} %bitcast.78), kind=kLoop, calls=%fused_computation.3 | loop fusion | flops 4194304 | bytes 4194304 | tf_op jit(solution)/shard_map/concatenate | solution.py:706
  84.8 0.0 copy-done.9
  84.8 0.2 copy-done.11
  85.0 0.1 copy-done.13
  85.2 38.2 %stick.1 = (bf16[512,512]{1,0:T(8,128)(2,1)S(1)}, bf16[4,512,512]{2,1,0:T(8,128)(2,1)S(1)}) custom-call(bf16[8,256,128]{2,1,0:T(8,128)(2,1)S(1)} %copy-done.13, bf16[8,512,128]{2,1,0:T(8,128)(2,1)S(1)} %copy-done.9, bf16[8,512,128]{2,1,0:T(8,128)(2,1)S(1)} %copy-done.11, bf16[8,16,128]{2,1,0:T(8,128)(2,1)S(1)} %get-tuple-element.15.bias_ref, ...), custom_call_target="tpu_custom_call" | custom-call | flops 4831838208 | bytes 2621440 | tf_op jit(solution)/shard_map/stick/pallas_call | solution.py:169
  123.4 0.0 copy-start.2
  123.4 0.3 convert_reduce_fusion
  123.7 0.5 copy-done.2
  124.2 0.8 slice.13
  125.0 27.8 %gather.1 = (bf16[512,2048]{1,0:T(8,128)(2,1)}, bf16[8,48,512]{2,1,0:T(8,128)(2,1)}) custom-call(bf16[512,512]{1,0:T(8,128)(2,1)} %copy-done.2, bf16[8,48,512]{2,1,0:T(8,128)(2,1)} %bitcast.77), custom_call_target="tpu_custom_call" | custom-call | bytes 26214400 | tf_op jit(solution)/shard_map/gather/pallas_call | solution.py:607
  152.8 0.0 copy-start.16
  152.8 0.0 copy-start.17
  152.8 4.3 %convolution_convert_fusion.2 = bf16[512,512]{1,0:T(8,128)(2,1)} fusion(bf16[512,2048]{1,0:T(8,128)(2,1)} %get-tuple-element.19, bf16[2048,512]{1,0:T(8,128)(2,1)} %copy-done.6), kind=kOutput, calls=%fused_computation.13 | convolution fusion | flops 1074003968 | bytes 4718592 | tf_op jit(solution)/shard_map/dot_general | solution.py:717
  157.1 0.0 copy-done.16
  157.1 0.0 copy-done.17
  157.1 0.2 convolution_add_fusion.1
  157.4 0.9 fusion.21
  (3 shorter events, 0.0 us)
Async XLA Ops:
  0.6 77.0 %copy-start = (bf16[1,512,2048]{2,1,0:T(8,128)(2,1)S(1)}, bf16[1,512,2048]{2,1,0:T(8,128)(2,1)}, u32[]{:S(2)}) copy-start(bf16[1,512,2048]{2,1,0:T(8,128)(2,1)} %param.29) | copy-start | bytes 6291460
  8.3 0.8 copy-start.14
  11.9 5.4 %copy-start.3 = (bf16[512,512]{1,0:T(8,128)(2,1)S(1)}, bf16[512,512]{1,0:T(8,128)(2,1)}, u32[]{:S(2)}) copy-start(bf16[512,512]{1,0:T(8,128)(2,1)} %query_ref.1) | copy-start | bytes 1572868
  11.9 5.4 %copy-start.4 = (bf16[512,512]{1,0:T(8,128)(2,1)S(1)}, bf16[512,512]{1,0:T(8,128)(2,1)}, u32[]{:S(2)}) copy-start(bf16[512,512]{1,0:T(8,128)(2,1)} %key_ref.1) | copy-start | bytes 1572868
  17.3 1.6 %copy-start.1 = (bf16[512,2048]{1,0:T(8,128)(2,1)S(1)}, bf16[512,2048]{1,0:T(8,128)(2,1)}, u32[]{:S(2)}) copy-start(bf16[512,2048]{1,0:T(8,128)(2,1)} %weight_ref.1) | copy-start | bytes 6291460
  18.9 1.0 copy-start.5
  19.9 55.9 %copy-start.18 = (bf16[1,2048,512]{2,1,0:T(8,128)(2,1)S(1)}, bf16[1,2048,512]{2,1,0:T(8,128)(2,1)}, u32[]{:S(2)}) copy-start(bf16[1,2048,512]{2,1,0:T(8,128)(2,1)} %param.27) | copy-start | bytes 6291460
  70.5 1.3 copy-start.6
  71.8 1.0 copy-start.8
  72.8 1.0 copy-start.10
  73.8 0.8 copy-start.12
  74.6 1.2 copy-start.7
  77.7 5.4 %copy-start.15 = (bf16[128,2048]{1,0:T(8,128)(2,1)S(1)}, bf16[128,2048]{1,0:T(8,128)(2,1)}, u32[]{:S(2)}) copy-start(bf16[128,2048]{1,0:T(8,128)(2,1)} %convolution_convert_fusion.1) | copy-start | bytes 1572868
  83.0 1.8 %copy-start.9 = (bf16[8,512,128]{2,1,0:T(8,128)(2,1)S(1)}, bf16[8,512,128]{2,1,0:T(8,128)(2,1)}, u32[]{:S(2)}) copy-start(bf16[8,512,128]{2,1,0:T(8,128)(2,1)} %copy-done.8) | copy-start | bytes 3145732
  83.0 2.0 %copy-start.11 = (bf16[8,512,128]{2,1,0:T(8,128)(2,1)S(1)}, bf16[8,512,128]{2,1,0:T(8,128)(2,1)}, u32[]{:S(2)}) copy-start(bf16[8,512,128]{2,1,0:T(8,128)(2,1)} %copy-done.10) | copy-start | bytes 3145732
  83.0 2.1 %copy-start.13 = (bf16[8,256,128]{2,1,0:T(8,128)(2,1)S(1)}, bf16[8,256,128]{2,1,0:T(8,128)(2,1)}, u32[]{:S(2)}) copy-start(bf16[8,256,128]{2,1,0:T(8,128)(2,1)} %copy-done.12) | copy-start | bytes 1572868
  123.4 0.8 copy-start.2
  152.8 4.3 %copy-start.16 = (bf16[8,48,512]{2,1,0:T(8,128)(2,1)S(1)}, bf16[8,48,512]{2,1,0:T(8,128)(2,1)}, u32[]{:S(2)}) copy-start(bf16[8,48,512]{2,1,0:T(8,128)(2,1)} %get-tuple-element.21) | copy-start | bytes 1179652
  152.8 4.3 %copy-start.17 = (bf16[384,128]{1,0:T(8,128)(2,1)S(1)}, bf16[384,128]{1,0:T(8,128)(2,1)}, u32[]{:S(2)}) copy-start(bf16[384,128]{1,0:T(8,128)(2,1)} %get-tuple-element.23) | copy-start | bytes 294916
